TPU v7x, 32 devices: a whole 2x2x4 slice. The times are simulated.
32 devices in a mesh: rep: 2 (over x), fs: 8 (over z, y), tp: 2 (over core).
Axes of the slice: x: 2, y: 2, z: 4, core: 2. Of those that a mesh axis runs over, the one named last changes fastest.
Arguments:
- tokens: bfloat16 [256, 16, 2048], P('tp', ('rep', 'fs')), may hold values from -6 to 6
- mix_gain: float32 [2048], replicated, may hold values from 0.1 to 1.9
- value_weight: bfloat16 [2048, 1024], P('fs', 'tp'), may hold values from -0.125 to 0.125
- gate_weight: bfloat16 [2048, 1024], P('fs', 'tp'), may hold values from -0.125 to 0.125
- conv_taps: float32 [31, 1024], P(None, 'tp'), may hold values from -1 to 1
- head_gain: float32 [1024], P('tp'), may hold values from 0.1 to 1.9
- out_weight: bfloat16 [1024, 2048], P('tp', 'fs'), may hold values from -0.1875 to 0.1875
- ffn_gain: float32 [2048], replicated, may hold values from 0.1 to 1.9
- ffn_gate_weight: bfloat16 [2048, 3072], P('fs', 'tp'), may hold values from -0.125 to 0.125
- ffn_up_weight: bfloat16 [2048, 3072], P('fs', 'tp'), may hold values from -0.125 to 0.125
- down_weight: bfloat16 [3072, 2048], P('tp', 'fs'), may hold values from -0.109375 to 0.109375
Outputs:
- layer_out: bfloat16 [256, 16, 2048], P('tp', ('rep', 'fs'))
All inputs are finite; a program needn't handle non-finite values.
Results may differ from a plain program's by a relative error of at most 0.012.
Values may be sent and summed in bfloat16 or wider, within the bound.
A program may use at most 128 MiB of HBM per device.

v0:
```python
import functools

import jax
import jax.numpy as jnp
from jax import lax
from jax.experimental import pallas as pl
from jax.experimental.pallas import tpu as pltpu
from jax.sharding import PartitionSpec as P

HEAD_DIM = 128
MESH = pl.DeviceIdType.MESH

norm_eps = 1e-06
group_eps = 1e-05
f32 = jnp.float32
bf16 = jnp.bfloat16


def rms_scale(matrix, scales):
    return matrix * lax.rsqrt(jnp.mean(matrix * matrix, axis=-1, keepdims=True) + norm_eps) * scales


class Moves:
    def __init__(self, n_rep, n_fs, sources, wholes, axes, sems):
        self.rep, self.fs, self.tp = lax.axis_index("rep"), lax.axis_index("fs"), lax.axis_index("tp")
        rep, fs, tp = self.rep, self.fs, self.tp
        self.ring = n_fs // 2
        self.pair, self.place = fs % 2, fs // 2
        flip = fs + 1 - 2 * self.pair
        self.to_tp = (rep, fs, 1 - tp)
        self.peers = (None, (rep, flip, tp), (1 - rep, fs, tp), (1 - rep, flip, tp))
        self.after = (rep, (fs + 2) % n_fs, tp)
        self.before = (rep, (fs + n_fs - 2) % n_fs, tp)
        self.quarter = rep * 2 + self.pair
        self.other = rep * 2 + 1 - self.pair
        self.sources, self.wholes, self.axes = sources, wholes, axes
        self.ring_send, self.ring_recv, self.pair_send, self.pair_recv = sems

    def barrier(self):
        sem = pltpu.get_barrier_semaphore()
        others = self.peers[1:] + (self.to_tp, self.after, self.before)
        for device in others:
            pl.semaphore_signal(sem, inc=1, device_id=device, device_id_type=MESH)
        pl.semaphore_wait(sem, len(others))

    def part(self, w, quarter):
        size = self.sources[w].shape[self.axes[w]] // 4
        at = pl.ds(pl.multiple_of(quarter * size, size), size)
        return (slice(None), at) if self.axes[w] == 1 else (at, slice(None))

    def slot(self, w, owner):
        if self.axes[w] == 0:
            return (owner,)
        size = self.sources[w].shape[0]
        return (pl.ds(pl.multiple_of(owner * size, size), size), slice(None))

    def pair_copy(self, w):
        return pltpu.make_async_remote_copy(
            src_ref=self.sources[w].at[self.part(w, self.other)],
            dst_ref=self.wholes[w].at[self.slot(w, self.fs)],
            send_sem=self.pair_send.at[w],
            recv_sem=self.pair_recv.at[w],
            device_id=self.peers[1],
            device_id_type=MESH,
        )

    def ring_copy(self, w, p, s):
        parity = self.pair if p == 0 else 1 - self.pair
        owner = ((self.place + self.ring + 1 - s) % self.ring) * 2 + parity
        there = self.wholes[w].at[self.slot(w, owner)]
        here = self.sources[w].at[self.part(w, self.quarter)] if s == 1 and p == 0 else there
        return pltpu.make_async_remote_copy(
            src_ref=here,
            dst_ref=there,
            send_sem=self.ring_send.at[w, p, s - 1],
            recv_sem=self.ring_recv.at[w, p, s - 1],
            device_id=self.after,
            device_id_type=MESH,
        )

    def push(self, w, p, s):
        if s > 1:
            self.ring_copy(w, p, s - 1).wait_recv()
        elif p == 1:
            self.pair_copy(w).wait_recv()
        self.ring_copy(w, p, s).start()

    def arrived(self, w):
        for p in (0, 1):
            self.ring_copy(w, p, self.ring - 1).wait_recv()

    def sent(self):
        for w in range(len(self.sources)):
            self.pair_copy(w).wait_send()
            for p in (0, 1):
                for s in range(1, self.ring):
                    self.ring_copy(w, p, s).wait_send()

    def copy(self, src, dst, device, sems, i):
        return pltpu.make_async_remote_copy(
            src_ref=src,
            dst_ref=dst,
            send_sem=sems[0].at[i],
            recv_sem=sems[1].at[i],
            device_id=device,
            device_id_type=MESH,
        )


class RowGather:
    def __init__(self, m, own, rows, sems):
        half = own.shape[0] // 2
        low, high = pl.ds(0, half), pl.ds(half, half)
        _, pair, rep, _ = m.peers
        moves = (
            (own.at[low], rows.at[2, low], rep),
            (own.at[high], rows.at[1, high], pair),
            (own.at[high], rows.at[2, high], rep),
            (own.at[low], rows.at[1, low], pair),
            (rows.at[2, low], rows.at[3, low], pair),
            (rows.at[1, high], rows.at[3, high], rep),
            (own, rows.at[4], m.to_tp),
            (rows.at[2], rows.at[6], m.to_tp),
            (rows.at[1], rows.at[5], m.to_tp),
            (rows.at[3, low], rows.at[7, low], m.to_tp),
            (rows.at[3, high], rows.at[7, high], m.to_tp),
        )
        self.copies = [m.copy(*move, sems, i) for i, move in enumerate(moves)]

    def start(self):
        for i in (0, 1, 2, 3, 6):
            self.copies[i].start()

    def forward(self):
        for i in (0, 1):
            self.copies[i].wait_recv()
            self.copies[i + 4].start()

    def finish(self):
        for i in (2, 3, 4, 5):
            self.copies[i].wait_recv()
            self.copies[i + 5].start()

    def arrived(self):
        for i in range(6, 11):
            self.copies[i].wait_recv()

    def sent(self):
        for copy in self.copies:
            copy.wait_send()


def ring_scratch(count, n_fs):
    ring = n_fs // 2
    return [pltpu.SemaphoreType.DMA((count, 2, ring - 1))] * 2 + [pltpu.SemaphoreType.DMA((count,))] * 2


def whole_shapes(weights, axes, n_fs):
    shapes = []
    for weight, axis in zip(weights, axes):
        shape = list(weight.shape)
        shape[axis] //= 4
        shapes.append((shape[0] * n_fs, shape[1]) if axis == 1 else (n_fs, *shape))
    return shapes


def first_kernel(
    n_rep, n_fs, own, value, gate, out, rows, value_q, gate_q, out_q,
    ring_send, ring_recv, pair_send, pair_recv, row_send, row_recv, local_sem,
):
    sems = (ring_send, ring_recv, pair_send, pair_recv)
    m = Moves(n_rep, n_fs, (value, gate, out), (value_q, gate_q, out_q), (1, 1, 0), sems)
    row_sems = (row_send, row_recv)
    local = [pltpu.make_async_copy(own, rows.at[0], local_sem.at[3])]
    for w in range(3):
        local.append(
            pltpu.make_async_copy(
                m.sources[w].at[m.part(w, m.quarter)],
                m.wholes[w].at[m.slot(w, m.fs)],
                local_sem.at[w],
            )
        )
    for copy in local:
        copy.start()
    m.barrier()
    for w in range(3):
        m.pair_copy(w).start()
        m.push(w, 0, 1)
    gather = RowGather(m, own, rows, row_sems)
    gather.start()
    for w in range(3):
        m.push(w, 1, 1)
    gather.forward()
    for s in range(2, m.ring):
        for p in (0, 1):
            for w in range(3):
                m.push(w, p, s)
    gather.finish()
    for w in range(3):
        m.arrived(w)
    gather.arrived()
    for copy in local:
        copy.wait()
    gather.sent()
    m.sent()


def second_kernel(
    n_rep, n_fs, tokens, act_near, act_far, out_q, ffn_gain, gate, up, down, result,
    gate_q, up_q, down_q, rows, hidden, middle, total, tp_out, tp_in, x_out, x_in,
    ring_send, ring_recv, pair_send, pair_recv, row_send, row_recv, sum_send, sum_recv,
):
    sems = (ring_send, ring_recv, pair_send, pair_recv)
    m = Moves(n_rep, n_fs, (gate, up, down), (gate_q, up_q, down_q), (1, 1, 0), sems)
    row_sems = (row_send, row_recv)
    length, width = tokens.shape
    tile = 512
    high = 32
    m.barrier()
    for w in range(3):
        m.pair_copy(w).start()
    for w in range(2):
        m.push(w, 0, 1)

    def columns(weight, c):
        slots = tile // weight.shape[2]
        return jnp.concatenate([weight[c * slots + i] for i in range(slots)], axis=1)

    def tile_loop(step):
        def run(c, _):
            step(columns(out_q, c), pl.ds(pl.multiple_of(c * tile, tile), tile))
            return _

        lax.fori_loop(0, width // tile, run, 0)

    def phase_columns(phase):
        if phase == 0:
            return slice(None)
        size = 2 * width // n_fs
        owner = (m.place + m.ring + 1 - phase) % m.ring
        return pl.ds(pl.multiple_of(owner * size, size), size)

    def for_columns(phase, step):
        if phase == 0:
            tile_loop(step)
        else:
            owner = ((m.place + m.ring + 1 - phase) % m.ring) * 2
            weight = jnp.concatenate([down_q[owner], down_q[owner + 1]], axis=1)
            step(weight, phase_columns(phase))

    def tp_copy(phase, k):
        b, at = min(phase, 1), phase_columns(phase)
        phase_sems = (sum_send.at[phase], sum_recv.at[phase])
        return m.copy(tp_out.at[b, k, :, at], tp_in.at[b, k, :, at], m.to_tp, phase_sems, k)

    def x_copy(phase, k, low):
        b, columns_at = min(phase, 1), phase_columns(phase)
        at = pl.ds(0, length // 2) if low else pl.ds(length // 2, length // 2)
        to_rep = k == 2 or (k == 3 and low)
        return m.copy(
            x_out.at[b, k - 1, at, columns_at],
            x_in.at[b, k - 1, at, columns_at],
            m.peers[2 if to_rep else 1],
            (sum_send.at[phase], sum_recv.at[phase]),
            2 * k + 2 + low,
        )

    def far_sums(phase, far):
        b = min(phase, 1)
        for k in (3, 2, 1, 0):

            def step(weight, at):
                product = jnp.dot(far(k), weight, preferred_element_type=f32)
                tp_out[b, k, :, at] = product.astype(bf16)

            for_columns(phase, step)
            tp_copy(phase, k).start()

    def near_sums(phase, near):
        b = min(phase, 1)
        for k in (3, 2, 1, 0):
            tp_copy(phase, k).wait_recv()

            def step(weight, at):
                part = jnp.dot(near(k), weight, preferred_element_type=f32)
                part = part + tp_in[b, k, :, at].astype(f32)
                if k == 0:
                    total[b, :, at] = part
                else:
                    x_out[b, k - 1, :, at] = part.astype(bf16)

            for_columns(phase, step)
            if k == 3:
                x_copy(phase, 3, 1).start()
                x_copy(phase, 3, 0).start()
            elif k:
                x_copy(phase, k, k - 1).start()

    def forward_sums(phase):
        b, columns_at = min(phase, 1), phase_columns(phase)
        for k, low in ((1, 1), (2, 0)):
            x_copy(phase, 3, low).wait_recv()
            first = 0 if low else length // 2

            def add(i, _):
                at = pl.ds(pl.multiple_of(first + i * high, high), high)
                part = x_out[b, k - 1, at, columns_at].astype(f32)
                part = part + x_in[b, 2, at, columns_at].astype(f32)
                x_out[b, k - 1, at, columns_at] = part.astype(bf16)
                return _

            lax.fori_loop(0, length // (2 * high), add, 0)
            x_copy(phase, k, low).start()

    def sums_arrived(phase):
        for k in (1, 2):
            for low in (0, 1):
                x_copy(phase, k, low).wait_recv()

    def all_sums(b, at):
        part = total[b, at, :]
        for k in (1, 2):
            part = part + x_in[b, k - 1, at, :].astype(f32)
        return part

    far_sums(0, lambda k: act_far[k])
    for w in range(2):
        m.push(w, 1, 1)
    near_sums(0, lambda k: act_near[k])
    for w in range(3):
        m.wholes[w][m.slot(w, m.fs)] = m.sources[w][m.part(w, m.quarter)]
    for w in range(2):
        m.push(w, 0, 2)
    forward_sums(0)
    for w in range(2):
        m.push(w, 1, 2)
    sums_arrived(0)

    def norm_rows(i, _):
        at = pl.ds(pl.multiple_of(i * high, high), high)
        mid = (tokens[at, :].astype(f32) + all_sums(0, at)).astype(bf16)
        middle[at, :] = mid
        rows[0, at, :] = rms_scale(mid.astype(f32), ffn_gain[...]).astype(bf16)
        return _

    lax.fori_loop(0, length // high, norm_rows, 0)
    gather = RowGather(m, rows.at[0], rows, row_sems)
    gather.start()
    for s in range(3, m.ring):
        for p in (0, 1):
            for w in range(2):
                m.push(w, p, s)
            if s == 3 and p == 0:
                gather.forward()
    if m.ring < 4:
        gather.forward()
    for p in (0, 1):
        m.push(2, p, 1)
    gather.finish()
    for w in range(2):
        m.arrived(w)
    m.push(2, 0, 2)
    gather.arrived()

    def feed(i, _):
        at = pl.ds(2 * i, 2)
        block = rows[at].reshape(2 * length, width)
        gate_part = jnp.dot(block, gate_q[...], preferred_element_type=f32)
        up_part = jnp.dot(block, up_q[...], preferred_element_type=f32)
        hidden[at] = (jax.nn.silu(gate_part) * up_part).astype(bf16).reshape(2, length, -1)
        return _

    lax.fori_loop(0, 4, feed, 0)
    m.push(2, 1, 2)
    for t in range(m.ring):
        if t == m.ring - 1:
            m.arrived(2)
        elif t > 1:
            for p in (0, 1):
                m.push(2, p, t + 1)
        far_sums(1 + t, lambda k: hidden[4 + k])
        near_sums(1 + t, lambda k: hidden[k])
        if t:
            forward_sums(t)
    forward_sums(m.ring)
    for t in range(m.ring):
        sums_arrived(1 + t)

    def finish(i, _):
        at = pl.ds(pl.multiple_of(i * high, high), high)
        result[at, :] = (middle[at, :].astype(f32) + all_sums(1, at)).astype(bf16)
        return _

    lax.fori_loop(0, length // high, finish, 0)
    gather.sent()
    for phase in range(1 + m.ring):
        for k in range(4):
            tp_copy(phase, k).wait_send()
        for k in (1, 2, 3):
            for low in (0, 1):
                x_copy(phase, k, low).wait_send()
    m.sent()


def body(
    tokens,
    mix_gain,
    value_weight,
    gate_weight,
    conv_taps,
    head_gain,
    out_weight,
    ffn_gain,
    ffn_gate_weight,
    ffn_up_weight,
    down_weight,
):
    n_rep, n_fs, n_tp = lax.axis_size("rep"), lax.axis_size("fs"), lax.axis_size("tp")
    rep, fs, tp = lax.axis_index("rep"), lax.axis_index("fs"), lax.axis_index("tp")
    pair = fs % 2
    local_len, seq_count, width = tokens.shape
    assert n_rep == 2 and n_tp == 2 and n_fs % 2 == 0 and seq_count == 1
    mine_q = rep * 2 + pair
    vmem, anywhere = pl.BlockSpec(memory_space=pltpu.VMEM), pl.BlockSpec(memory_space=pl.ANY)
    sem = pltpu.SemaphoreType.DMA

    rows = tokens.reshape(local_len, width)
    own = rms_scale(rows.astype(f32), mix_gain).astype(bf16)
    module_weights = (value_weight, gate_weight, out_weight)
    shapes = whole_shapes(module_weights, (1, 1, 0), n_fs)
    normed, value_q, gate_q, out_q = pl.pallas_call(
        functools.partial(first_kernel, n_rep, n_fs),
        out_shape=[jax.ShapeDtypeStruct(s, bf16) for s in [(8, local_len, width)] + shapes],
        in_specs=[vmem] * 4,
        out_specs=[anywhere] * 4,
        scratch_shapes=ring_scratch(3, n_fs) + [sem((11,)), sem((11,)), sem((4,))],
        compiler_params=pltpu.CompilerParams(collective_id=0, has_side_effects=True),
    )(own, *module_weights)
    normed = normed.reshape(8 * local_len, width)

    value_rows = jnp.dot(normed, value_q, preferred_element_type=f32)
    gate_rows = jnp.dot(normed, gate_q, preferred_element_type=f32)
    glu = (value_rows * jax.nn.sigmoid(gate_rows)).astype(bf16)
    channels = glu.shape[1]
    glu = glu.reshape(2, 4, local_len, channels)
    first = jnp.where(tp == 0, glu[0], glu[1])
    second = jnp.where(tp == 0, glu[1], glu[0])
    sequence = jnp.concatenate([first, second], axis=1)
    taps = lax.dynamic_slice_in_dim(conv_taps, mine_q * channels, channels, 1)
    gains = lax.dynamic_slice_in_dim(head_gain, mine_q * channels, channels, 0)
    kernel = taps.shape[0]
    conved = lax.conv_general_dilated(
        sequence.astype(f32),
        taps[:, None, :],
        (1,),
        [(kernel // 2, kernel // 2)],
        dimension_numbers=("NWC", "WIO", "NWC"),
        feature_group_count=channels,
        precision=lax.Precision.HIGHEST,
    )
    grouped = conved.reshape(4, 2 * local_len, channels // HEAD_DIM, HEAD_DIM)
    head_mean = jnp.mean(grouped, axis=-1, keepdims=True)
    head_var = jnp.mean(jnp.square(grouped - head_mean), axis=-1, keepdims=True)
    scaled = (grouped - head_mean) * lax.rsqrt(head_var + group_eps) * gains.reshape(-1, HEAD_DIM)
    activated = jax.nn.silu(scaled).astype(bf16).reshape(4, 2 * local_len, channels)
    near = lax.dynamic_slice_in_dim(activated, tp * local_len, local_len, 1)
    far = lax.dynamic_slice_in_dim(activated, (1 - tp) * local_len, local_len, 1)
    ffn_weights = (ffn_gate_weight, ffn_up_weight, down_weight)
    shapes = whole_shapes(ffn_weights, (1, 1, 0), n_fs)
    units = shapes[0][1]
    layer_rows = pl.pallas_call(
        functools.partial(second_kernel, n_rep, n_fs),
        out_shape=jax.ShapeDtypeStruct((local_len, width), bf16),
        in_specs=[vmem] * 8,
        out_specs=vmem,
        scratch_shapes=[pltpu.VMEM(s, bf16) for s in shapes]
        + [
            pltpu.VMEM((8, local_len, width), bf16),
            pltpu.VMEM((8, local_len, units), bf16),
            pltpu.VMEM((local_len, width), bf16),
            pltpu.VMEM((2, local_len, width), f32),
            pltpu.VMEM((2, 4, local_len, width), bf16),
            pltpu.VMEM((2, 4, local_len, width), bf16),
            pltpu.VMEM((2, 3, local_len, width), bf16),
            pltpu.VMEM((2, 3, local_len, width), bf16),
        ]
        + ring_scratch(3, n_fs)
        + [sem((11,)), sem((11,)), sem((1 + n_fs // 2, 10)), sem((1 + n_fs // 2, 10))],
        compiler_params=pltpu.CompilerParams(
            collective_id=1, has_side_effects=True, vmem_limit_bytes=56 * 1024 * 1024
        ),
    )(rows, near, far, out_q, ffn_gain.reshape(1, width), *ffn_weights)
    return layer_rows.reshape(local_len, seq_count, width)


def solution(mesh):
    placed = (
        P("tp", ("rep", "fs"), None),
        P(),
        P("fs", "tp"),
        P("fs", "tp"),
        P(None, "tp"),
        P("tp"),
        P("tp", "fs"),
        P(),
        P("fs", "tp"),
        P("fs", "tp"),
        P("tp", "fs"),
    )
    return jax.shard_map(
        body, mesh=mesh, in_specs=placed, out_specs=P("tp", ("rep", "fs"), None), check_vma=False
    )
```

profile of v0, /device:TPU:0, one launch (start us, length us, event | category | flops | bytes accessed | tf_op | source)
XLA Modules:
  0.0 147.2 jit_solution(884289334190769585)
XLA Ops:
  0.0 0.0 copy-start
  0.0 0.8 copy-done
  0.9 1.2 fusion.4
  2.1 2.0 %fusion.6.own = bf16[128,2048]{1,0:T(8,128)(2,1)} fusion(f32[2048]{0:T(1024)} %param.12, f32[128]{0:T(128)S(1)} %add_rsqrt_fusion.1, bf16[128,1,2048]{2,0,1:T(8,128)(2,1)} %param.11), kind=kLoop, calls=%fused_computation.10 | loop fusion | flops 1048576 | bytes 1057280 | tf_op jit(solution)/shard_map/convert_element_type | solution.py:428
  4.1 37.4 %shard_map.109 = (bf16[8,128,2048]{2,1,0:T(8,128)(2,1)}, bf16[2048,128]{1,0:T(8,128)(2,1)}, bf16[2048,128]{1,0:T(8,128)(2,1)}, bf16[8,128,256]{2,1,0:T(8,128)(2,1)}) custom-call(bf16[128,2048]{1,0:T(8,128)(2,1)} %fusion.6.own, bf16[256,512]{1,0:T(8,128)(2,1)} %value.1, bf16[256,512]{1,0:T(8,128)(2,1)} %gate.2, bf16[512,256]{1,0:T(8,128)(2,1)} %out.1), custom_call_target="tpu_custom_call" | custom-call | tf_op jit(solution)/shard_map/pallas_call | solution.py:431
  41.5 0.0 copy-start.1
  41.5 0.0 copy-start.2
  41.5 3.7 %fusion.2 = f32[1024,128]{1,0:T(8,128)S(1)} fusion(bf16[1024,2048]{1,0:T(8,128)(2,1)} %bitcast.13, bf16[2048,128]{1,0:T(8,128)(2,1)} %get-tuple-element.11), kind=kOutput, calls=%fused_computation.6 | convolution fusion | flops 537264128 | bytes 5242880 | tf_op jit(solution)/shard_map/dot_general | solution.py:442
  45.2 0.0 copy-done.1
  45.3 0.0 copy-done.2
  45.3 1.2 fusion.3
  46.6 0.1 copy.26
  46.7 0.1 copy.27
  46.8 3.2 %fusion.12 = (f32[4,256]{0,1:T(8,128)S(1)}, f32[4,256,128]{2,0,1:T(4,128)S(1)}) fusion(f32[31,1,128]{2,1,0:T(1,128)S(1)} %broadcast_in_dim.2, bf16[4,128,128]{2,0,1:T(4,128)(2,1)S(1)} %copy.27, bf16[4,128,128]{2,0,1:T(4,128)(2,1)S(1)} %copy.26), kind=kOutput, calls=%fused_computation.27 | convolution fusion | flops 47938560 | bytes 806400 | tf_op jit(solution)/shard_map/conv_general_dilated | solution.py:452
  50.0 0.1 copy.28
  50.0 0.4 multiply_reduce_fusion
  50.4 0.8 dynamic_slice.13
  51.2 0.4 multiply_convert_fusion
  51.6 0.7 constant_dynamic-slice_fusion
  52.3 93.0 %shard_map.110 = bf16[128,2048]{1,0:T(8,128)(2,1)} custom-call(bf16[128,2048]{1,0:T(8,128)(2,1)} %bitcast.15, bf16[4,128,128]{2,1,0:T(8,128)(2,1)} %get-tuple-element.14.act_near, bf16[4,128,128]{2,1,0:T(8,128)(2,1)} %get-tuple-element.13.act_far, bf16[8,128,256]{2,1,0:T(8,128)(2,1)} %get-tuple-element.12.out_q, f32[1,2048]{1,0:T(1,128)} %bitcast.19, ...), custom_call_target="tpu_custom_call" | custom-call | tf_op jit(solution)/shard_map/pallas_call | solution.py:471
  145.3 1.9 %copy.36 = bf16[128,1,2048]{2,0,1:T(8,128)(2,1)} copy(bf16[128,1,2048]{2,0,1:T(8,128)(2,1)} %bitcast.16) | data formatting | bytes 1048576
  (6 shorter events, 0.1 us)
Async XLA Ops:
  0.0 0.8 copy-start
  41.5 3.7 %copy-start.1 = (bf16[8,128,2048]{2,1,0:T(8,128)(2,1)S(1)}, bf16[8,128,2048]{2,1,0:T(8,128)(2,1)}, u32[]{:S(2)}) copy-start(bf16[8,128,2048]{2,1,0:T(8,128)(2,1)} %get-tuple-element.9) | copy-start | bytes 12582916
  41.5 3.7 %copy-start.2 = (bf16[2048,128]{1,0:T(8,128)(2,1)S(1)}, bf16[2048,128]{1,0:T(8,128)(2,1)}, u32[]{:S(2)}) copy-start(bf16[2048,128]{1,0:T(8,128)(2,1)} %get-tuple-element.10) | copy-start | bytes 1572868
where the time goes:
time: 148 us; the launch traced here: 147 us
  Pallas kernels  130 us (88%)
  matrix products  8.12 us (5%)
  local copies, waits for them, and re-layouts  4.51 us (3%)
  other arithmetic  4.07 us (3%)
    pallas_call x1, Pallas kernels, body(): pl.pallas_call(functools.partial(second_kernel, n_rep, n_fs), out_shape=j...  93 us
    pallas_call x1, Pallas kernels, body(): pl.pallas_call(functools.partial(first_kernel, n_rep, n_fs), out_shape=[j...  37.4 us
    dot_general x1, matrix products, body(): gate_rows = jnp.dot(normed, gate_q, preferred_element_type=f32)  3.71 us
    conv_general_dilated x1, matrix products, body(): lax.conv_general_dilated(sequence.astype(f32), taps[:, None, :], (1,), [(...  3.17 us

commit v1 on v0

v1 whole, which is shorter than its diff:
```python
import functools

import jax
import jax.numpy as jnp
from jax import lax
from jax.experimental import pallas as pl
from jax.experimental.pallas import tpu as pltpu
from jax.sharding import PartitionSpec as P

HEAD_DIM = 128
MESH = pl.DeviceIdType.MESH

norm_eps = 1e-06
group_eps = 1e-05
f32 = jnp.float32
bf16 = jnp.bfloat16


def rms_scale(matrix, scales):
    return matrix * lax.rsqrt(jnp.mean(matrix * matrix, axis=-1, keepdims=True) + norm_eps) * scales


class Moves:
    def __init__(self, n_rep, n_fs, sources, wholes, offsets, axes, sems):
        self.rep, self.fs, self.tp = lax.axis_index("rep"), lax.axis_index("fs"), lax.axis_index("tp")
        rep, fs, tp = self.rep, self.fs, self.tp
        self.ring = n_fs // 2
        self.pair, self.place = fs % 2, fs // 2
        flip = fs + 1 - 2 * self.pair
        self.to_tp = (rep, fs, 1 - tp)
        self.peers = (None, (rep, flip, tp), (1 - rep, fs, tp), (1 - rep, flip, tp))
        self.after = (rep, (fs + 2) % n_fs, tp)
        self.before = (rep, (fs + n_fs - 2) % n_fs, tp)
        self.quarter = rep * 2 + self.pair
        self.other = rep * 2 + 1 - self.pair
        self.sources, self.wholes, self.offsets, self.axes = sources, wholes, offsets, axes
        self.ring_send, self.ring_recv, self.pair_send, self.pair_recv = sems

    def greet(self):
        for device in self.peers[1:] + (self.to_tp, self.after, self.before):
            pl.semaphore_signal(pltpu.get_barrier_semaphore(), inc=1, device_id=device, device_id_type=MESH)

    def meet(self):
        pl.semaphore_wait(pltpu.get_barrier_semaphore(), 6)

    def part(self, w, quarter):
        size = self.sources[w].shape[self.axes[w]] // 4
        at = pl.ds(pl.multiple_of(quarter * size, size), size)
        return (slice(None), at) if self.axes[w] == 1 else (at, slice(None))

    def slot(self, w, owner):
        if self.axes[w] == 0:
            return (owner,)
        size, columns = self.sources[w].shape
        at = pl.ds(pl.multiple_of(owner * size, size), size)
        return (at, pl.ds(self.offsets[w], columns // 4))

    def pair_copy(self, w):
        return pltpu.make_async_remote_copy(
            src_ref=self.sources[w].at[self.part(w, self.other)],
            dst_ref=self.wholes[w].at[self.slot(w, self.fs)],
            send_sem=self.pair_send.at[w],
            recv_sem=self.pair_recv.at[w],
            device_id=self.peers[1],
            device_id_type=MESH,
        )

    def ring_copy(self, w, p, s):
        parity = self.pair if p == 0 else 1 - self.pair
        owner = ((self.place + self.ring + 1 - s) % self.ring) * 2 + parity
        there = self.wholes[w].at[self.slot(w, owner)]
        here = self.sources[w].at[self.part(w, self.quarter)] if s == 1 and p == 0 else there
        return pltpu.make_async_remote_copy(
            src_ref=here,
            dst_ref=there,
            send_sem=self.ring_send.at[w, p, s - 1],
            recv_sem=self.ring_recv.at[w, p, s - 1],
            device_id=self.after,
            device_id_type=MESH,
        )

    def push(self, w, p, s):
        if s > 1:
            self.ring_copy(w, p, s - 1).wait_recv()
        elif p == 1:
            self.pair_copy(w).wait_recv()
        self.ring_copy(w, p, s).start()

    def arrived(self, w):
        for p in (0, 1):
            self.ring_copy(w, p, self.ring - 1).wait_recv()

    def sent(self):
        for w in range(len(self.sources)):
            self.pair_copy(w).wait_send()
            for p in (0, 1):
                for s in range(1, self.ring):
                    self.ring_copy(w, p, s).wait_send()

    def copy(self, src, dst, device, sems, i):
        return pltpu.make_async_remote_copy(
            src_ref=src,
            dst_ref=dst,
            send_sem=sems[0].at[i],
            recv_sem=sems[1].at[i],
            device_id=device,
            device_id_type=MESH,
        )


class RowGather:
    def __init__(self, m, own, rows, sems):
        half = own.shape[0] // 2
        low, high = pl.ds(0, half), pl.ds(half, half)
        _, pair, rep, _ = m.peers
        first, near_pair, near_rep, across = (2 * k + m.tp for k in range(4))
        moves = (
            (own.at[low], rows.at[near_rep, low], rep),
            (own.at[high], rows.at[near_pair, high], pair),
            (own.at[high], rows.at[near_rep, high], rep),
            (own.at[low], rows.at[near_pair, low], pair),
            (rows.at[near_rep, low], rows.at[across, low], pair),
            (rows.at[near_pair, high], rows.at[across, high], rep),
            (own, rows.at[first], m.to_tp),
            (rows.at[near_rep], rows.at[near_rep], m.to_tp),
            (rows.at[near_pair], rows.at[near_pair], m.to_tp),
            (rows.at[across, low], rows.at[across, low], m.to_tp),
            (rows.at[across, high], rows.at[across, high], m.to_tp),
        )
        self.copies = [m.copy(*move, sems, i) for i, move in enumerate(moves)]

    def start(self):
        for i in (0, 1, 2, 3, 6):
            self.copies[i].start()

    def forward(self):
        for i in (0, 1):
            self.copies[i].wait_recv()
            self.copies[i + 4].start()

    def finish(self):
        for i in (2, 3, 4, 5):
            self.copies[i].wait_recv()
            self.copies[i + 5].start()

    def ready(self, k):
        for i in ((6,), (8,), (7,), (9, 10))[k]:
            self.copies[i].wait_recv()

    def sent(self):
        for copy in self.copies:
            copy.wait_send()


VALUE, GATE, OUT, FFN_GATE, FFN_UP, DOWN = range(6)
AXES = (1, 1, 0, 1, 1, 0)


def layer_kernel(
    n_rep, n_fs, tokens_in, mix_gain_in, value, gate, taps_in, head_gain_in, out, ffn_gain_in, ffn_gate, ffn_up,
    down, result,
    *scratch,
):
    staged, scratch = scratch[:6], scratch[6:]
    module_q, out_q, ffn_q, down_q = scratch[:4]
    tokens, mix_gain, taps, head_gain, ffn_gain = scratch[4:9]
    rows_a, rows, padded, activated, hidden, middle, total, tp_out, tp_in, x_out, x_in, finished = scratch[9:21]
    ring_sems, scratch = scratch[21:25], scratch[25:]
    row_a_sems, row_sems, (sum_send, sum_recv), local_sem = scratch[:2], scratch[2:4], scratch[4:6], scratch[6]
    shards = (value, gate, out, ffn_gate, ffn_up, down)
    channels, units = out_q.shape[1], down_q.shape[1]
    wholes = (module_q, module_q, out_q, ffn_q, ffn_q, down_q)
    m = Moves(n_rep, n_fs, staged, wholes, (0, channels, None, 0, units, None), AXES, ring_sems)
    length, width = tokens.shape
    kernel = taps.shape[0]
    pad = (padded.shape[1] - 2 * length) // 2
    tile = 512
    high = 32
    near_at = pl.ds(pl.multiple_of(m.tp * length, length), length)
    far_at = pl.ds(pl.multiple_of((1 - m.tp) * length, length), length)

    local = [pltpu.make_async_copy(s, d, local_sem.at[i]) for i, (s, d) in enumerate(zip(shards, staged))]
    smalls = ((tokens_in, tokens), (mix_gain_in, mix_gain), (taps_in, taps))
    smalls += ((head_gain_in, head_gain), (ffn_gain_in, ffn_gain))
    small = [pltpu.make_async_copy(s, d, local_sem.at[6 + i]) for i, (s, d) in enumerate(smalls)]
    placed = []
    for w in range(6):
        placed.append(
            pltpu.make_async_copy(shards[w].at[m.part(w, m.quarter)], wholes[w].at[m.slot(w, m.fs)], local_sem.at[11 + w])
        )
    m.greet()
    for copy in local[:3] + small[:2] + placed[:2] + small[2:4] + placed[2:3] + local[3:] + placed[3:] + small[4:]:
        copy.start()
    for w in (VALUE, GATE, OUT):
        local[w].wait()
    m.meet()
    for w in (VALUE, GATE, OUT):
        m.pair_copy(w).start()
    for w in (VALUE, GATE, OUT):
        m.push(w, 0, 1)

    def module_norm(i, _):
        at = pl.ds(pl.multiple_of(i * high, high), high)
        rows_a[m.tp, at, :] = rms_scale(tokens[at, :].astype(f32), mix_gain[...]).astype(bf16)
        return _

    small[0].wait()
    small[1].wait()
    lax.fori_loop(0, length // high, module_norm, 0)
    gather = RowGather(m, rows_a.at[m.tp], rows_a, row_a_sems)
    gather.start()
    for w in (VALUE, GATE, OUT):
        m.push(w, 1, 1)
    for w in (FFN_GATE, FFN_UP, DOWN):
        local[w].wait()
    zeros = jnp.zeros((4, pad, channels), f32)
    padded[:, pl.ds(0, pad), :] = zeros
    padded[:, pl.ds(pad + 2 * length, pad), :] = zeros
    for s in range(2, m.ring):
        for p in (0, 1):
            for w in (VALUE, GATE, OUT):
                m.push(w, p, s)
        if s == 2:
            gather.forward()
    for w in (FFN_GATE, FFN_UP):
        m.pair_copy(w).start()
    for w in (FFN_GATE, FFN_UP):
        m.push(w, 0, 1)
    gather.finish()
    for copy in placed + small[2:]:
        copy.wait()
    m.arrived(VALUE)
    m.arrived(GATE)

    def gated(k):
        block = rows_a[pl.ds(2 * k, 2)].reshape(2 * length, width)
        both = jnp.dot(block, module_q[...], preferred_element_type=f32)
        glu = (both[:, :channels] * jax.nn.sigmoid(both[:, channels:])).astype(bf16)
        padded[k, pl.ds(pad, 2 * length), :] = glu.astype(f32)

    channels_at = pl.ds(pl.multiple_of(m.quarter * channels, channels), channels)
    conv_rows = 64

    def convolve(k, _):
        for first in range(0, 2 * length, conv_rows):
            conved = jnp.zeros((conv_rows, channels), f32)
            for t in range(kernel):
                shifted = padded[k, pl.ds(first + t + pad - kernel // 2, conv_rows), :]
                conved = conved + shifted * taps[pl.ds(t, 1), channels_at]
            gains = head_gain[:, channels_at]
            for g in range(0, channels, HEAD_DIM):
                grouped = conved[:, g : g + HEAD_DIM]
                head_mean = jnp.mean(grouped, axis=-1, keepdims=True)
                head_var = jnp.mean(jnp.square(grouped - head_mean), axis=-1, keepdims=True)
                scaled = (grouped - head_mean) * lax.rsqrt(head_var + group_eps) * gains[:, g : g + HEAD_DIM]
                activated[k, pl.ds(first, conv_rows), pl.ds(g, HEAD_DIM)] = jax.nn.silu(scaled).astype(bf16)
        return _

    for k in range(4):
        gather.ready(k)
        gated(k)
    lax.fori_loop(0, 4, convolve, 0)
    m.arrived(OUT)

    def columns(weight, c):
        slots = tile // weight.shape[2]
        return jnp.concatenate([weight[c * slots + i] for i in range(slots)], axis=1)

    def tile_loop(step):
        def run(c, _):
            step(columns(out_q, c), pl.ds(pl.multiple_of(c * tile, tile), tile))
            return _

        lax.fori_loop(0, width // tile, run, 0)

    def phase_columns(phase):
        if phase == 0:
            return slice(None)
        size = 2 * width // n_fs
        owner = (m.place + m.ring + 1 - phase) % m.ring
        return pl.ds(pl.multiple_of(owner * size, size), size)

    def for_columns(phase, step):
        if phase == 0:
            tile_loop(step)
        else:
            owner = ((m.place + m.ring + 1 - phase) % m.ring) * 2
            weight = jnp.concatenate([down_q[owner], down_q[owner + 1]], axis=1)
            step(weight, phase_columns(phase))

    def tp_copy(phase, k):
        b, at = min(phase, 1), phase_columns(phase)
        phase_sems = (sum_send.at[phase], sum_recv.at[phase])
        return m.copy(tp_out.at[b, k, :, at], tp_in.at[b, k, :, at], m.to_tp, phase_sems, k)

    def x_copy(phase, k, low):
        b, columns_at = min(phase, 1), phase_columns(phase)
        at = pl.ds(0, length // 2) if low else pl.ds(length // 2, length // 2)
        to_rep = k == 2 or (k == 3 and low)
        return m.copy(
            x_out.at[b, k - 1, at, columns_at],
            x_in.at[b, k - 1, at, columns_at],
            m.peers[2 if to_rep else 1],
            (sum_send.at[phase], sum_recv.at[phase]),
            2 * k + 2 + low,
        )

    def far_sums(phase, far):
        b = min(phase, 1)
        for k in (3, 2, 1, 0):

            def step(weight, at):
                product = jnp.dot(far(k), weight, preferred_element_type=f32)
                tp_out[b, k, :, at] = product.astype(bf16)

            for_columns(phase, step)
            tp_copy(phase, k).start()

    def near_sums(phase, near):
        b = min(phase, 1)
        for k in (3, 2, 1, 0):
            tp_copy(phase, k).wait_recv()

            def step(weight, at):
                part = jnp.dot(near(k), weight, preferred_element_type=f32)
                part = part + tp_in[b, k, :, at].astype(f32)
                if k == 0:
                    total[b, :, at] = part
                else:
                    x_out[b, k - 1, :, at] = part.astype(bf16)

            for_columns(phase, step)
            if k == 3:
                x_copy(phase, 3, 1).start()
                x_copy(phase, 3, 0).start()
            elif k:
                x_copy(phase, k, k - 1).start()

    def forward_sums(phase):
        b, columns_at = min(phase, 1), phase_columns(phase)
        for k, low in ((1, 1), (2, 0)):
            x_copy(phase, 3, low).wait_recv()
            first = 0 if low else length // 2

            def add(i, _):
                at = pl.ds(pl.multiple_of(first + i * high, high), high)
                part = x_out[b, k - 1, at, columns_at].astype(f32)
                part = part + x_in[b, 2, at, columns_at].astype(f32)
                x_out[b, k - 1, at, columns_at] = part.astype(bf16)
                return _

            lax.fori_loop(0, length // (2 * high), add, 0)
            x_copy(phase, k, low).start()

    def sums_arrived(phase):
        for k in (1, 2):
            for low in (0, 1):
                x_copy(phase, k, low).wait_recv()

    def all_sums(b, at):
        part = total[b, at, :]
        for k in (1, 2):
            part = part + x_in[b, k - 1, at, :].astype(f32)
        return part

    far_sums(0, lambda k: activated[k, far_at, :])
    for w in (FFN_GATE, FFN_UP):
        m.push(w, 1, 1)
    near_sums(0, lambda k: activated[k, near_at, :])
    for w in (FFN_GATE, FFN_UP):
        m.push(w, 0, 2)
    forward_sums(0)
    for w in (FFN_GATE, FFN_UP):
        m.push(w, 1, 2)
    m.pair_copy(DOWN).start()
    sums_arrived(0)

    def norm_rows(i, _):
        at = pl.ds(pl.multiple_of(i * high, high), high)
        mid = (tokens[at, :].astype(f32) + all_sums(0, at)).astype(bf16)
        middle[at, :] = mid
        rows[m.tp, at, :] = rms_scale(mid.astype(f32), ffn_gain[...]).astype(bf16)
        return _

    lax.fori_loop(0, length // high, norm_rows, 0)
    ffn_gather = RowGather(m, rows.at[m.tp], rows, row_sems)
    ffn_gather.start()
    for s in range(3, m.ring):
        for p in (0, 1):
            for w in (FFN_GATE, FFN_UP):
                m.push(w, p, s)
            if s == 3 and p == 0:
                ffn_gather.forward()
    if m.ring < 4:
        ffn_gather.forward()
    for p in (0, 1):
        m.push(DOWN, p, 1)
    ffn_gather.finish()
    for k in range(4):
        ffn_gather.ready(k)
    m.arrived(FFN_GATE)
    m.arrived(FFN_UP)

    def feed(i, _):
        at = pl.ds(2 * i, 2)
        block = rows[at].reshape(2 * length, width)
        both = jnp.dot(block, ffn_q[...], preferred_element_type=f32)
        hidden[at] = (jax.nn.silu(both[:, :units]) * both[:, units:]).astype(bf16).reshape(2, length, -1)
        return _

    lax.fori_loop(0, 4, feed, 0)
    for t in range(m.ring):
        if t and t == m.ring - 1:
            m.arrived(DOWN)
        elif t:
            for p in (0, 1):
                m.push(DOWN, p, t + 1)
        far_sums(1 + t, lambda k: hidden[2 * k + 1 - m.tp])
        near_sums(1 + t, lambda k: hidden[2 * k + m.tp])
        if t:
            forward_sums(t)
    forward_sums(m.ring)
    for t in range(m.ring):
        sums_arrived(1 + t)

    def finish(i, _):
        at = pl.ds(pl.multiple_of(i * high, high), high)
        finished[at, :] = (middle[at, :].astype(f32) + all_sums(1, at)).astype(bf16)
        return _

    lax.fori_loop(0, length // high, finish, 0)
    leave = pltpu.make_async_copy(finished, result, local_sem.at[17])
    leave.start()
    gather.sent()
    ffn_gather.sent()
    for phase in range(1 + m.ring):
        for k in range(4):
            tp_copy(phase, k).wait_send()
        for k in (1, 2, 3):
            for low in (0, 1):
                x_copy(phase, k, low).wait_send()
    m.sent()
    leave.wait()


def body(
    tokens,
    mix_gain,
    value_weight,
    gate_weight,
    conv_taps,
    head_gain,
    out_weight,
    ffn_gain,
    ffn_gate_weight,
    ffn_up_weight,
    down_weight,
):
    n_rep, n_fs, n_tp = lax.axis_size("rep"), lax.axis_size("fs"), lax.axis_size("tp")
    length, seq_count, width = tokens.shape
    assert n_rep == 2 and n_tp == 2 and n_fs % 2 == 0 and n_fs > 4 and seq_count == 1
    ring = n_fs // 2
    kernel = conv_taps.shape[0]
    channels, units = out_weight.shape[0] // 4, down_weight.shape[0] // 4
    pad = -(-(kernel // 2) // 8) * 8
    sem = pltpu.SemaphoreType.DMA
    weights = (value_weight, gate_weight, out_weight, ffn_gate_weight, ffn_up_weight, down_weight)
    operands = (
        tokens.reshape(length, width),
        mix_gain.reshape(1, width),
        value_weight,
        gate_weight,
        conv_taps,
        head_gain.reshape(1, -1),
        out_weight,
        ffn_gain.reshape(1, width),
        ffn_gate_weight,
        ffn_up_weight,
        down_weight,
    )
    layer_rows = pl.pallas_call(
        functools.partial(layer_kernel, n_rep, n_fs),
        out_shape=jax.ShapeDtypeStruct((length, width), bf16),
        in_specs=[pl.BlockSpec(memory_space=pl.ANY)] * len(operands),
        out_specs=pl.BlockSpec(memory_space=pl.ANY),
        scratch_shapes=[pltpu.VMEM(w.shape, bf16) for w in weights]
        + [
            pltpu.VMEM((width, 2 * channels), bf16),
            pltpu.VMEM((n_fs, channels, out_weight.shape[1]), bf16),
            pltpu.VMEM((width, 2 * units), bf16),
            pltpu.VMEM((n_fs, units, down_weight.shape[1]), bf16),
            pltpu.VMEM((length, width), bf16),
            pltpu.VMEM((1, width), f32),
            pltpu.VMEM(conv_taps.shape, f32),
            pltpu.VMEM((1, head_gain.shape[0]), f32),
            pltpu.VMEM((1, width), f32),
            pltpu.VMEM((8, length, width), bf16),
            pltpu.VMEM((8, length, width), bf16),
            pltpu.VMEM((4, 2 * length + 2 * pad, channels), f32),
            pltpu.VMEM((4, 2 * length, channels), bf16),
            pltpu.VMEM((8, length, units), bf16),
            pltpu.VMEM((length, width), bf16),
            pltpu.VMEM((2, length, width), f32),
            pltpu.VMEM((2, 4, length, width), bf16),
            pltpu.VMEM((2, 4, length, width), bf16),
            pltpu.VMEM((2, 3, length, width), bf16),
            pltpu.VMEM((2, 3, length, width), bf16),
            pltpu.VMEM((length, width), bf16),
        ]
        + [sem((6, 2, ring - 1)), sem((6, 2, ring - 1)), sem((6,)), sem((6,))]
        + [sem((11,)), sem((11,)), sem((11,)), sem((11,))]
        + [sem((1 + ring, 10)), sem((1 + ring, 10)), sem((18,))],
        compiler_params=pltpu.CompilerParams(
            collective_id=0, has_side_effects=True, vmem_limit_bytes=60 * 1024 * 1024
        ),
    )(*operands)
    return layer_rows.reshape(length, seq_count, width)


def solution(mesh):
    placed = (
        P("tp", ("rep", "fs"), None),
        P(),
        P("fs", "tp"),
        P("fs", "tp"),
        P(None, "tp"),
        P("tp"),
        P("tp", "fs"),
        P(),
        P("fs", "tp"),
        P("fs", "tp"),
        P("tp", "fs"),
    )
    return jax.shard_map(
        body, mesh=mesh, in_specs=placed, out_specs=P("tp", ("rep", "fs"), None), check_vma=False
    )
```

time: 148 us -> 124 us (0.84)
  matrix products: 8.12 us -> 0 us
  Pallas kernels: 130 us -> 122 us
  other arithmetic: 4.07 us -> 0 us
  local copies, waits for them, and re-layouts: 4.51 us -> 1.88 us
    pallas_call x2 -> x1, Pallas kernels: 130 us -> 122 us  [body(): pl.pallas_call(functools.partial(layer_kernel, n_rep, n_fs), out_shape=ja...]
    dot_general x2 -> x0, matrix products: 4.95 us -> none  [the longest x1 3.71 us: body(): gate_rows = jnp.dot(normed, gate_q, preferred_element_type=f32)]
    conv_general_dilated x1 -> x0, matrix products: 3.17 us -> none  [body(): lax.conv_general_dilated(sequence.astype(f32), taps[:, None, :], (1,), [(...]
    convert_element_type x2 -> x0, other arithmetic: 2.4 us -> none  [the longest x1 2.04 us: body(): own = rms_scale(rows.astype(f32), mix_gain).astype(bf16)]
    reduce_sum x2 -> x0, other arithmetic: 1.63 us -> none  [the longest x1 1.23 us: rms_scale(): jnp.mean(matrix * matrix, axis=-1, keepdims=True) + norm_eps]
    dynamic_slice x3 -> x0, local copies, waits for them, and re-layouts: 1.49 us -> none  [the longest x1 0.76 us: body(): gains = lax.dynamic_slice_in_dim(head_gain, mine_q * channels, channels, 0)]
where the time goes in v1:
time: 124 us
  Pallas kernels  122 us (98%)
  local copies, waits for them, and re-layouts  1.88 us (2%)
    pallas_call x1, Pallas kernels, body(): pl.pallas_call(functools.partial(layer_kernel, n_rep, n_fs), out_shape=ja...  122 us

profile of v1, /device:TPU:0, one launch (start us, length us, event | category | flops | bytes accessed | tf_op | source)
XLA Modules:
  0.0 123.9 jit_solution(16386865031090505101)
XLA Ops:
  0.0 122.0 %shard_map.109 = bf16[128,2048]{1,0:T(8,128)(2,1)} custom-call(bf16[128,2048]{1,0:T(8,128)(2,1)} %bitcast.6, f32[1,2048]{1,0:T(1,128)} %bitcast.7, bf16[256,512]{1,0:T(8,128)(2,1)} %value.1, bf16[256,512]{1,0:T(8,128)(2,1)} %gate.1, f32[31,512]{1,0:T(8,128)} %taps_in.1, f32[1,512]{1,0:T(1,128)} %bitcast.9, bf16[512,256]{1,0:T(8,128)(2,1)} %out.1, ...), custom_call_target="tpu_custom_call" | custom-call | tf_op jit(solution)/shard_map/pallas_call | solution.py:481
  122.0 1.9 %copy.13 = bf16[128,1,2048]{2,0,1:T(8,128)(2,1)} copy(bf16[128,1,2048]{2,0,1:T(8,128)(2,1)} %bitcast.5) | data formatting | bytes 1048576

commit v2 on v1

v2 whole, which is shorter than its diff:
```python
import functools

import jax
import jax.numpy as jnp
from jax import lax
from jax.experimental import pallas as pl
from jax.experimental.pallas import tpu as pltpu
from jax.sharding import PartitionSpec as P

HEAD_DIM = 128
MESH = pl.DeviceIdType.MESH

norm_eps = 1e-06
group_eps = 1e-05
f32 = jnp.float32
bf16 = jnp.bfloat16


def rms_scale(matrix, scales):
    return matrix * lax.rsqrt(jnp.mean(matrix * matrix, axis=-1, keepdims=True) + norm_eps) * scales


MODULE, OUT, FFN, DOWN = range(4)


class Moves:
    def __init__(self, n_rep, n_fs, sources, wholes, axes, sems):
        self.rep, self.fs, self.tp = lax.axis_index("rep"), lax.axis_index("fs"), lax.axis_index("tp")
        rep, fs, tp = self.rep, self.fs, self.tp
        self.n_fs, self.ring = n_fs, n_fs // 2
        self.pair, self.place = fs % 2, fs // 2
        flip = fs + 1 - 2 * self.pair
        self.to_tp = (rep, fs, 1 - tp)
        self.peers = (None, (rep, flip, tp), (1 - rep, fs, tp), (1 - rep, flip, tp))
        self.after = (rep, (fs + 2) % n_fs, tp)
        self.before = (rep, (fs + n_fs - 2) % n_fs, tp)
        self.quarter = rep * 2 + self.pair
        self.other = rep * 2 + 1 - self.pair
        self.sources, self.wholes, self.axes = sources, wholes, axes
        self.send, self.ring_recv, self.pair_recv = sems

    def greet(self):
        for device in self.peers[1:] + (self.to_tp, self.after, self.before):
            pl.semaphore_signal(pltpu.get_barrier_semaphore(), inc=1, device_id=device, device_id_type=MESH)

    def meet(self):
        pl.semaphore_wait(pltpu.get_barrier_semaphore(), 6)

    def part(self, w, quarter):
        size = self.sources[w].shape[self.axes[w]] // 4
        at = pl.ds(pl.multiple_of(quarter * size, size), size)
        return (slice(None), at) if self.axes[w] == 1 else (at, slice(None))

    def slots(self, w, owner, count=1):
        if self.axes[w] == 0:
            return (owner,) if count == 1 else (pl.ds(owner, count),)
        size = self.sources[w].shape[0]
        return (pl.ds(pl.multiple_of(owner * size, size), count * size), slice(None))

    def copy(self, src, dst, device, send_sem, recv_sem):
        return pltpu.make_async_remote_copy(
            src_ref=src,
            dst_ref=dst,
            send_sem=send_sem,
            recv_sem=recv_sem,
            device_id=device,
            device_id_type=MESH,
        )

    def pair_copy(self, w):
        source, there = self.sources[w].at[self.part(w, self.other)], self.wholes[w].at[self.slots(w, self.fs)]
        return self.copy(source, there, self.peers[1], self.send.at[w], self.pair_recv.at[w])

    def ring_copy(self, w, p, s):
        parity = p if w == DOWN else self.pair if p == 0 else 1 - self.pair
        owner = ((self.place + self.ring + 1 - s) % self.ring) * 2 + parity
        there = self.wholes[w].at[self.slots(w, owner)]
        here = self.sources[w].at[self.part(w, self.quarter)] if w != DOWN and s == 1 and p == 0 else there
        return self.copy(here, there, self.after, self.send.at[w], self.ring_recv.at[w, p, s - 1])

    def push(self, w, p, s):
        if s > 1:
            self.ring_copy(w, p, s - 1).wait_recv()
        elif p == (0 if w == DOWN else 1):
            self.pair_copy(w).wait_recv()
        self.ring_copy(w, p, s).start()

    def arrived(self, w):
        for p in (0, 1):
            self.ring_copy(w, p, self.ring - 1).wait_recv()

    def sent(self, w):
        all_sent = self.wholes[w].at[self.slots(w, 0, self.n_fs - 1)]
        self.copy(all_sent, all_sent, self.after, self.send.at[w], self.pair_recv.at[w]).wait_send()


class RowGather:
    def __init__(self, m, rows, send_sem, recv_sems):
        half = rows.shape[1] // 2
        low, high = pl.ds(0, half), pl.ds(half, half)
        _, pair, rep, _ = m.peers
        first, near_pair, near_rep, across = (2 * k + m.tp for k in range(4))
        moves = (
            (rows.at[first, low], rows.at[near_rep, low], rep),
            (rows.at[first, high], rows.at[near_pair, high], pair),
            (rows.at[first, high], rows.at[near_rep, high], rep),
            (rows.at[first, low], rows.at[near_pair, low], pair),
            (rows.at[near_rep, low], rows.at[across, low], pair),
            (rows.at[near_pair, high], rows.at[across, high], rep),
            (rows.at[first], rows.at[first], m.to_tp),
            (rows.at[near_rep], rows.at[near_rep], m.to_tp),
            (rows.at[near_pair], rows.at[near_pair], m.to_tp),
            (rows.at[across, low], rows.at[across, low], m.to_tp),
            (rows.at[across, high], rows.at[across, high], m.to_tp),
        )
        self.copies = [m.copy(*move, send_sem, recv_sems.at[i]) for i, move in enumerate(moves)]
        seven = rows.at[pl.ds(0, 7)]
        self.all_sent = m.copy(seven, seven, pair, send_sem, recv_sems.at[0])

    def start(self):
        for i in (0, 1, 2, 3, 6):
            self.copies[i].start()

    def forward(self):
        for i in (0, 1):
            self.copies[i].wait_recv()
            self.copies[i + 4].start()

    def finish(self):
        for i in (2, 3, 4, 5):
            self.copies[i].wait_recv()
            self.copies[i + 5].start()

    def ready(self, k):
        for i in ((6,), (8,), (7,), (9, 10))[k]:
            self.copies[i].wait_recv()

    def sent(self):
        self.all_sent.wait_send()


def layer_kernel(
    n_rep, n_fs, tokens_in, mix_gain_in, value, gate, taps_in, head_gain_in, out, ffn_gain_in, ffn_gate, ffn_up,
    down, result,
    *scratch,
):
    staged, wholes, scratch = scratch[:4], scratch[4:8], scratch[8:]
    module_q, out_q, ffn_q, down_q = wholes
    tokens, mix_gain, taps, head_gain, ffn_gain = scratch[:5]
    rows_a, rows, padded, activated, hidden, middle, total, tp_out, tp_in, x_out, x_in, finished = scratch[5:17]
    weight_sems, scratch = scratch[17:20], scratch[20:]
    row_send, row_recv, tp_send, tp_recv, x_send, x_first, x_last, stage_sem, place_sem, small_sem, end_sem = scratch
    channels, units = out_q.shape[1], down_q.shape[1]
    m = Moves(n_rep, n_fs, staged, wholes, (1, 0, 1, 0), weight_sems)
    length, width = tokens.shape
    kernel = taps.shape[0]
    pad = (padded.shape[1] - 2 * length) // 2
    tile = 512
    high = 32
    near_at = pl.ds(pl.multiple_of(m.tp * length, length), length)
    far_at = pl.ds(pl.multiple_of((1 - m.tp) * length, length), length)

    def stage(w, shards):
        if len(shards) == 1:
            pltpu.make_async_copy(shards[0], staged[w], stage_sem.at[w]).start()
            return
        size = shards[0].shape[1] // 4
        for i, shard in enumerate(shards):
            for q in range(4):
                there = staged[w].at[:, pl.ds((2 * q + i) * size, size)]
                pltpu.make_async_copy(shard.at[:, pl.ds(q * size, size)], there, stage_sem.at[w]).start()

    def stage_wait(w):
        pltpu.make_async_copy(staged[w], staged[w], stage_sem.at[w]).wait()

    def place(w, wait):
        there = wholes[w].at[m.slots(w, m.fs)]
        copy = pltpu.make_async_copy(staged[w].at[m.part(w, m.quarter)], there, place_sem.at[w])
        copy.wait() if wait else copy.start()

    smalls = ((tokens_in, tokens), (mix_gain_in, mix_gain), (taps_in, taps))
    smalls += ((head_gain_in, head_gain), (ffn_gain_in, ffn_gain))
    small = [pltpu.make_async_copy(s, d, small_sem.at[i]) for i, (s, d) in enumerate(smalls)]
    m.greet()
    stage(MODULE, (value, gate))
    stage(OUT, (out,))
    small[0].start()
    small[1].start()
    stage(FFN, (ffn_gate, ffn_up))
    stage(DOWN, (down,))
    for copy in small[2:]:
        copy.start()
    stage_wait(MODULE)
    m.meet()
    m.pair_copy(MODULE).start()
    m.push(MODULE, 0, 1)
    stage_wait(OUT)
    m.pair_copy(OUT).start()
    m.push(OUT, 0, 1)

    def module_norm(i, _):
        at = pl.ds(pl.multiple_of(i * high, high), high)
        rows_a[m.tp, at, :] = rms_scale(tokens[at, :].astype(f32), mix_gain[...]).astype(bf16)
        return _

    small[0].wait()
    small[1].wait()
    lax.fori_loop(0, length // high, module_norm, 0)
    gather = RowGather(m, rows_a, row_send, row_recv)
    gather.start()
    m.push(MODULE, 1, 1)
    m.push(OUT, 1, 1)
    for w in (FFN, DOWN):
        stage_wait(w)
    for w in (MODULE, OUT, FFN, DOWN):
        place(w, False)
    zeros = jnp.zeros((4, pad, channels), f32)
    padded[:, pl.ds(0, pad), :] = zeros
    padded[:, pl.ds(pad + 2 * length, pad), :] = zeros
    for s in range(2, m.ring):
        for p in (0, 1):
            m.push(MODULE, p, s)
            m.push(OUT, p, s)
            if s == 2 and p == 0:
                gather.forward()
    m.pair_copy(FFN).start()
    m.push(FFN, 0, 1)
    gather.finish()
    for w in (MODULE, OUT, FFN, DOWN):
        place(w, True)
    for copy in small[2:]:
        copy.wait()
    m.arrived(MODULE)

    def gated(k):
        block = rows_a[pl.ds(2 * k, 2)].reshape(2 * length, width)
        both = jnp.dot(block, module_q[...], preferred_element_type=f32)
        glu = (both[:, :channels] * jax.nn.sigmoid(both[:, channels:])).astype(bf16)
        padded[k, pl.ds(pad, 2 * length), :] = glu.astype(f32)

    channels_at = pl.ds(pl.multiple_of(m.quarter * channels, channels), channels)
    conv_rows = 64

    def convolve(k, _):
        for first in range(0, 2 * length, conv_rows):
            conved = jnp.zeros((conv_rows, channels), f32)
            for t in range(kernel):
                shifted = padded[k, pl.ds(first + t + pad - kernel // 2, conv_rows), :]
                conved = conved + shifted * taps[pl.ds(t, 1), channels_at]
            gains = head_gain[:, channels_at]
            for g in range(0, channels, HEAD_DIM):
                grouped = conved[:, g : g + HEAD_DIM]
                head_mean = jnp.mean(grouped, axis=-1, keepdims=True)
                head_var = jnp.mean(jnp.square(grouped - head_mean), axis=-1, keepdims=True)
                scaled = (grouped - head_mean) * lax.rsqrt(head_var + group_eps) * gains[:, g : g + HEAD_DIM]
                activated[k, pl.ds(first, conv_rows), pl.ds(g, HEAD_DIM)] = jax.nn.silu(scaled).astype(bf16)
        return _

    for k in range(4):
        gather.ready(k)
        gated(k)
    lax.fori_loop(0, 4, convolve, 0)
    m.push(FFN, 1, 1)
    m.arrived(OUT)

    def columns(weight, c):
        slots = tile // weight.shape[2]
        return jnp.concatenate([weight[c * slots + i] for i in range(slots)], axis=1)

    def tile_loop(step):
        def run(c, _):
            step(columns(out_q, c), pl.ds(pl.multiple_of(c * tile, tile), tile))
            return _

        lax.fori_loop(0, width // tile, run, 0)

    size = down_q.shape[2]
    halved = size % 128 == 0
    phases = [None] + [(t, None) for t in range(m.ring - 1)]
    phases += [(m.ring - 1, 0), (m.ring - 1, 1)] if halved else [(m.ring - 1, None)]

    def phase_owner(phase):
        t, p = phases[phase]
        base = ((m.place + m.ring - t) % m.ring) * 2
        if p is None:
            return base, 2
        return base + p, 1

    def phase_columns(phase):
        if phase == 0:
            return slice(None)
        owner, count = phase_owner(phase)
        return pl.ds(pl.multiple_of(owner * size, count * size), count * size)

    def for_columns(phase, step):
        if phase == 0:
            tile_loop(step)
        else:
            owner, count = phase_owner(phase)
            weight = jnp.concatenate([down_q[owner + i] for i in range(count)], axis=1)
            step(weight, phase_columns(phase))

    def tp_copy(phase, k, count=1):
        b, at = min(phase, 1), (pl.ds(k, count), slice(None), phase_columns(phase))
        recv_sem = tp_recv.at[phase, 0 if k == 3 else 1]
        return m.copy(tp_out.at[(b, *at)], tp_in.at[(b, *at)], m.to_tp, tp_send.at[b], recv_sem)

    def x_copy(phase, k, low):
        b, columns_at = min(phase, 1), phase_columns(phase)
        at = pl.ds(0, length // 2) if low else pl.ds(length // 2, length // 2)
        to_rep = k == 2 or (k == 3 and low)
        there = (b, k - 1, at, columns_at)
        recv_sem = x_first.at[phase, low] if k == 3 else x_last.at[b]
        return m.copy(x_out.at[there], x_in.at[there], m.peers[2 if to_rep else 1], x_send.at[b], recv_sem)

    def far_sums(phase, far):
        b = min(phase, 1)
        for k in (3, 2, 1, 0):

            def step(weight, at):
                product = jnp.dot(far(k), weight, preferred_element_type=f32)
                tp_out[b, k, :, at] = product.astype(bf16)

            for_columns(phase, step)
            tp_copy(phase, k).start()

    def near_sums(phase, near):
        b = min(phase, 1)
        for k in (3, 2, 1, 0):
            if k == 3:
                tp_copy(phase, 3).wait_recv()
            elif k == 2:
                tp_copy(phase, 0, 3).wait_recv()

            def step(weight, at):
                part = jnp.dot(near(k), weight, preferred_element_type=f32)
                part = part + tp_in[b, k, :, at].astype(f32)
                if k == 0:
                    total[b, :, at] = part
                else:
                    x_out[b, k - 1, :, at] = part.astype(bf16)

            for_columns(phase, step)
            if k == 3:
                x_copy(phase, 3, 1).start()
                x_copy(phase, 3, 0).start()
            elif k:
                x_copy(phase, k, k - 1).start()

    def forward_sums(phase):
        b, columns_at = min(phase, 1), phase_columns(phase)
        for k, low in ((1, 1), (2, 0)):
            x_copy(phase, 3, low).wait_recv()
            first = 0 if low else length // 2

            def add(i, _):
                at = pl.ds(pl.multiple_of(first + i * high, high), high)
                part = x_out[b, k - 1, at, columns_at].astype(f32)
                part = part + x_in[b, 2, at, columns_at].astype(f32)
                x_out[b, k - 1, at, columns_at] = part.astype(bf16)
                return _

            lax.fori_loop(0, length // (2 * high), add, 0)
            x_copy(phase, k, low).start()

    def sums_arrived(b):
        both = x_in.at[b, pl.ds(0, 2)]
        m.copy(both, both, m.peers[1], x_send.at[b], x_last.at[b]).wait_recv()

    def sums_sent(b):
        m.copy(tp_out.at[b], tp_out.at[b], m.to_tp, tp_send.at[b], x_last.at[b]).wait_send()
        m.copy(x_out.at[b], x_out.at[b], m.peers[1], x_send.at[b], x_last.at[b]).wait_send()

    def all_sums(b, at):
        part = total[b, at, :]
        for k in (1, 2):
            part = part + x_in[b, k - 1, at, :].astype(f32)
        return part

    far_sums(0, lambda k: activated[k, far_at, :])
    near_sums(0, lambda k: activated[k, near_at, :])
    m.push(FFN, 0, 2)
    forward_sums(0)
    m.push(FFN, 1, 2)
    m.pair_copy(DOWN).start()
    gather.sent()
    sums_arrived(0)

    def norm_rows(i, _):
        at = pl.ds(pl.multiple_of(i * high, high), high)
        mid = (tokens[at, :].astype(f32) + all_sums(0, at)).astype(bf16)
        middle[at, :] = mid
        rows[m.tp, at, :] = rms_scale(mid.astype(f32), ffn_gain[...]).astype(bf16)
        return _

    lax.fori_loop(0, length // high, norm_rows, 0)
    gather = RowGather(m, rows, row_send, row_recv)
    gather.start()
    for s in range(3, m.ring):
        for p in (0, 1):
            m.push(FFN, p, s)
            if s == 3 and p == 0:
                gather.forward()
    if m.ring < 4:
        gather.forward()
    for p in (0, 1):
        m.push(DOWN, p, 1)
    gather.finish()
    for k in range(4):
        gather.ready(k)
    m.arrived(FFN)

    def feed(i, _):
        at = pl.ds(2 * i, 2)
        block = rows[at].reshape(2 * length, width)
        both = jnp.dot(block, ffn_q[...], preferred_element_type=f32)
        hidden[at] = (jax.nn.silu(both[:, :units]) * both[:, units:]).astype(bf16).reshape(2, length, -1)
        return _

    lax.fori_loop(0, 4, feed, 0)
    m.push(DOWN, 0, 2)
    for phase in range(1, len(phases)):
        t, p = phases[phase]
        for q in (0, 1) if p is None else (p,):
            if t == m.ring - 1:
                m.ring_copy(DOWN, q, t).wait_recv()
            elif t and (t, q) != (1, 0):
                m.push(DOWN, q, t + 1)
        far_sums(phase, lambda k: hidden[2 * k + 1 - m.tp])
        near_sums(phase, lambda k: hidden[2 * k + m.tp])
        if phase > 1:
            forward_sums(phase - 1)
    forward_sums(len(phases) - 1)
    sums_arrived(1)

    def finish(i, _):
        at = pl.ds(pl.multiple_of(i * high, high), high)
        finished[at, :] = (middle[at, :].astype(f32) + all_sums(1, at)).astype(bf16)
        return _

    lax.fori_loop(0, length // high, finish, 0)
    leave = pltpu.make_async_copy(finished, result, end_sem)
    leave.start()
    gather.sent()
    for b in (0, 1):
        sums_sent(b)
    for w in (MODULE, OUT, FFN, DOWN):
        m.sent(w)
    leave.wait()


def body(
    tokens,
    mix_gain,
    value_weight,
    gate_weight,
    conv_taps,
    head_gain,
    out_weight,
    ffn_gain,
    ffn_gate_weight,
    ffn_up_weight,
    down_weight,
):
    n_rep, n_fs, n_tp = lax.axis_size("rep"), lax.axis_size("fs"), lax.axis_size("tp")
    length, seq_count, width = tokens.shape
    assert n_rep == 2 and n_tp == 2 and n_fs % 2 == 0 and n_fs > 4 and seq_count == 1
    ring = n_fs // 2
    kernel = conv_taps.shape[0]
    channels, units = out_weight.shape[0] // 4, down_weight.shape[0] // 4
    pad = -(-(kernel // 2) // 8) * 8
    sem = pltpu.SemaphoreType.DMA
    operands = (
        tokens.reshape(length, width),
        mix_gain.reshape(1, width),
        value_weight,
        gate_weight,
        conv_taps,
        head_gain.reshape(1, -1),
        out_weight,
        ffn_gain.reshape(1, width),
        ffn_gate_weight,
        ffn_up_weight,
        down_weight,
    )
    layer_rows = pl.pallas_call(
        functools.partial(layer_kernel, n_rep, n_fs),
        out_shape=jax.ShapeDtypeStruct((length, width), bf16),
        in_specs=[pl.BlockSpec(memory_space=pl.ANY)] * len(operands),
        out_specs=pl.BlockSpec(memory_space=pl.ANY),
        scratch_shapes=[
            pltpu.VMEM((value_weight.shape[0], 8 * channels), bf16),
            pltpu.VMEM(out_weight.shape, bf16),
            pltpu.VMEM((ffn_gate_weight.shape[0], 8 * units), bf16),
            pltpu.VMEM(down_weight.shape, bf16),
            pltpu.VMEM((width, 2 * channels), bf16),
            pltpu.VMEM((n_fs, channels, out_weight.shape[1]), bf16),
            pltpu.VMEM((width, 2 * units), bf16),
            pltpu.VMEM((n_fs, units, down_weight.shape[1]), bf16),
            pltpu.VMEM((length, width), bf16),
            pltpu.VMEM((1, width), f32),
            pltpu.VMEM(conv_taps.shape, f32),
            pltpu.VMEM((1, head_gain.shape[0]), f32),
            pltpu.VMEM((1, width), f32),
            pltpu.VMEM((8, length, width), bf16),
            pltpu.VMEM((8, length, width), bf16),
            pltpu.VMEM((4, 2 * length + 2 * pad, channels), f32),
            pltpu.VMEM((4, 2 * length, channels), bf16),
            pltpu.VMEM((8, length, units), bf16),
            pltpu.VMEM((length, width), bf16),
            pltpu.VMEM((2, length, width), f32),
            pltpu.VMEM((2, 4, length, width), bf16),
            pltpu.VMEM((2, 4, length, width), bf16),
            pltpu.VMEM((2, 3, length, width), bf16),
            pltpu.VMEM((2, 3, length, width), bf16),
            pltpu.VMEM((length, width), bf16),
        ]
        + [sem((4,)), sem((4, 2, ring - 1)), sem((4,))]
        + [sem, sem((11,)), sem((2,)), sem((ring + 2, 2)), sem((2,)), sem((ring + 2, 2)), sem((2,))]
        + [sem((4,)), sem((4,)), sem((5,)), sem],
        compiler_params=pltpu.CompilerParams(
            collective_id=0, has_side_effects=True, vmem_limit_bytes=60 * 1024 * 1024
        ),
    )(*operands)
    return layer_rows.reshape(length, seq_count, width)


def solution(mesh):
    placed = (
        P("tp", ("rep", "fs"), None),
        P(),
        P("fs", "tp"),
        P("fs", "tp"),
        P(None, "tp"),
        P("tp"),
        P("tp", "fs"),
        P(),
        P("fs", "tp"),
        P("fs", "tp"),
        P("tp", "fs"),
    )
    return jax.shard_map(
        body, mesh=mesh, in_specs=placed, out_specs=P("tp", ("rep", "fs"), None), check_vma=False
    )
```

time: 124 us -> 121 us (0.976)
  Pallas kernels: 122 us -> 119 us
    pallas_call x1, Pallas kernels: 122 us -> 119 us  [body(): pl.pallas_call(functools.partial(layer_kernel, n_rep, n_fs), out_shape=ja...]
where the time goes in v2:
time: 121 us
  Pallas kernels  119 us (98%)
  local copies, waits for them, and re-layouts  1.88 us (2%)
    pallas_call x1, Pallas kernels, body(): pl.pallas_call(functools.partial(layer_kernel, n_rep, n_fs), out_shape=ja...  119 us

profile of v2, /device:TPU:0, one launch (start us, length us, event | category | flops | bytes accessed | tf_op | source)
XLA Modules:
  0.0 120.6 jit_solution(9661327540170594619)
XLA Ops:
  0.0 118.7 %shard_map.109 = bf16[128,2048]{1,0:T(8,128)(2,1)} custom-call(bf16[128,2048]{1,0:T(8,128)(2,1)} %bitcast.6, f32[1,2048]{1,0:T(1,128)} %bitcast.7, bf16[256,512]{1,0:T(8,128)(2,1)} %value.1, bf16[256,512]{1,0:T(8,128)(2,1)} %gate.1, f32[31,512]{1,0:T(8,128)} %taps_in.1, f32[1,512]{1,0:T(1,128)} %bitcast.9, bf16[512,256]{1,0:T(8,128)(2,1)} %out.1, ...), custom_call_target="tpu_custom_call" | custom-call | tf_op jit(solution)/shard_map/pallas_call | solution.py:486
  118.7 1.9 %copy.13 = bf16[128,1,2048]{2,0,1:T(8,128)(2,1)} copy(bf16[128,1,2048]{2,0,1:T(8,128)(2,1)} %bitcast.5) | data formatting | bytes 1048576

commit v3 on v2

--- a/solution.py
+++ b/solution.py
@@ -37,7 +37,8 @@
         self.quarter = rep * 2 + self.pair
         self.other = rep * 2 + 1 - self.pair
         self.sources, self.wholes, self.axes = sources, wholes, axes
-        self.send, self.ring_recv, self.pair_recv = sems
+        self.send, self.ring_recv, self.piece_recv, self.pair_recv = sems
+        self.pieces = max(1, wholes[DOWN].shape[2] // 128)
 
     def greet(self):
         for device in self.peers[1:] + (self.to_tp, self.after, self.before):
@@ -71,6 +72,13 @@
         source, there = self.sources[w].at[self.part(w, self.other)], self.wholes[w].at[self.slots(w, self.fs)]
         return self.copy(source, there, self.peers[1], self.send.at[w], self.pair_recv.at[w])
 
+    def piece_copy(self, i):
+        columns = self.wholes[DOWN].shape[2] // self.pieces
+        owner = ((self.place + 2) % self.ring) * 2 + 1
+        there = self.wholes[DOWN].at[owner, :, pl.ds(i * columns, columns)]
+        recv_sem = self.piece_recv.at[i]
+        return self.copy(there, there, self.after, self.send.at[DOWN], recv_sem)
+
     def ring_copy(self, w, p, s):
         parity = p if w == DOWN else self.pair if p == 0 else 1 - self.pair
         owner = ((self.place + self.ring + 1 - s) % self.ring) * 2 + parity
@@ -78,12 +86,23 @@
         here = self.sources[w].at[self.part(w, self.quarter)] if w != DOWN and s == 1 and p == 0 else there
         return self.copy(here, there, self.after, self.send.at[w], self.ring_recv.at[w, p, s - 1])
 
+    def push_own_ffn(self, lead):
+        rows = self.sources[FFN].shape[0]
+        at = pl.ds(0, rows // 4) if lead else pl.ds(rows // 4, rows - rows // 4)
+        there = self.wholes[FFN].at[self.slots(FFN, self.fs)].at[at, :]
+        here = self.sources[FFN].at[self.part(FFN, self.quarter)].at[at, :]
+        self.copy(here, there, self.after, self.send.at[FFN], self.ring_recv.at[FFN, 0, 0]).start()
+
     def push(self, w, p, s):
         if s > 1:
             self.ring_copy(w, p, s - 1).wait_recv()
         elif p == (0 if w == DOWN else 1):
             self.pair_copy(w).wait_recv()
-        self.ring_copy(w, p, s).start()
+        if (w, p, s) == (DOWN, 1, self.ring - 1):
+            for i in range(self.pieces):
+                self.piece_copy(i).start()
+        else:
+            self.ring_copy(w, p, s).start()
 
     def arrived(self, w):
         for p in (0, 1):
@@ -148,8 +167,8 @@
     module_q, out_q, ffn_q, down_q = wholes
     tokens, mix_gain, taps, head_gain, ffn_gain = scratch[:5]
     rows_a, rows, padded, activated, hidden, middle, total, tp_out, tp_in, x_out, x_in, finished = scratch[5:17]
-    weight_sems, scratch = scratch[17:20], scratch[20:]
-    row_send, row_recv, tp_send, tp_recv, x_send, x_first, x_last, stage_sem, place_sem, small_sem, end_sem = scratch
+    weight_sems, scratch = scratch[17:21], scratch[21:]
+    row_send, row_recv, tp_send, tp_recv, x_send, x_first, x_last, stage_sem, small_sem, end_sem = scratch
     channels, units = out_q.shape[1], down_q.shape[1]
     m = Moves(n_rep, n_fs, staged, wholes, (1, 0, 1, 0), weight_sems)
     length, width = tokens.shape
@@ -175,7 +194,7 @@
 
     def place(w, wait):
         there = wholes[w].at[m.slots(w, m.fs)]
-        copy = pltpu.make_async_copy(staged[w].at[m.part(w, m.quarter)], there, place_sem.at[w])
+        copy = pltpu.make_async_copy(staged[w].at[m.part(w, m.quarter)], there, stage_sem.at[w])
         copy.wait() if wait else copy.start()
 
     smalls = ((tokens_in, tokens), (mix_gain_in, mix_gain), (taps_in, taps))
@@ -197,6 +216,8 @@
     stage_wait(OUT)
     m.pair_copy(OUT).start()
     m.push(OUT, 0, 1)
+    stage_wait(FFN)
+    m.push_own_ffn(True)
 
     def module_norm(i, _):
         at = pl.ds(pl.multiple_of(i * high, high), high)
@@ -209,22 +230,24 @@
     gather = RowGather(m, rows_a, row_send, row_recv)
     gather.start()
     m.push(MODULE, 1, 1)
-    m.push(OUT, 1, 1)
-    for w in (FFN, DOWN):
-        stage_wait(w)
+    stage_wait(DOWN)
     for w in (MODULE, OUT, FFN, DOWN):
         place(w, False)
     zeros = jnp.zeros((4, pad, channels), f32)
     padded[:, pl.ds(0, pad), :] = zeros
     padded[:, pl.ds(pad + 2 * length, pad), :] = zeros
     for s in range(2, m.ring):
-        for p in (0, 1):
-            m.push(MODULE, p, s)
-            m.push(OUT, p, s)
-            if s == 2 and p == 0:
-                gather.forward()
-    m.pair_copy(FFN).start()
-    m.push(FFN, 0, 1)
+        m.push(MODULE, 0, s)
+        if s > 2:
+            m.push(OUT, 0, s - 1)
+        m.push(OUT, 1, s - 1)
+        m.push(MODULE, 1, s)
+        if s == 2:
+            gather.forward()
+            m.pair_copy(FFN).start()
+    for p in (0, 1):
+        m.push(OUT, p, m.ring - 1)
+    m.push_own_ffn(False)
     gather.finish()
     for w in (MODULE, OUT, FFN, DOWN):
         place(w, True)
@@ -259,8 +282,8 @@
     for k in range(4):
         gather.ready(k)
         gated(k)
+    m.push(FFN, 1, 1)
     lax.fori_loop(0, 4, convolve, 0)
-    m.push(FFN, 1, 1)
     m.arrived(OUT)
 
     def columns(weight, c):
@@ -275,34 +298,35 @@
         lax.fori_loop(0, width // tile, run, 0)
 
     size = down_q.shape[2]
-    halved = size % 128 == 0
-    phases = [None] + [(t, None) for t in range(m.ring - 1)]
-    phases += [(m.ring - 1, 0), (m.ring - 1, 1)] if halved else [(m.ring - 1, None)]
-
-    def phase_owner(phase):
-        t, p = phases[phase]
-        base = ((m.place + m.ring - t) % m.ring) * 2
-        if p is None:
-            return base, 2
-        return base + p, 1
+    last_t = m.ring - 1
+    phases = [None] + [(t, 0, 2 * size) for t in range(last_t)]
+    if size % 128 == 0:
+        phases += [(last_t, 0, size)] + [(last_t, size + c, 128) for c in range(0, size, 128)]
+    else:
+        phases += [(last_t, 0, 2 * size)]
+    final = len(phases) - 1
+    direct = [i for i in range(1, final + 1) if phases[i][0] == last_t and (phases[i][1] or i == final)]
+    final_count = sum(phases[i][2] for i in direct)
+
+    def phase_base(phase):
+        return ((m.place + m.ring - phases[phase][0]) % m.ring) * 2
 
     def phase_columns(phase):
         if phase == 0:
             return slice(None)
-        owner, count = phase_owner(phase)
-        return pl.ds(pl.multiple_of(owner * size, count * size), count * size)
-
-    def for_columns(phase, step):
-        if phase == 0:
-            tile_loop(step)
-        else:
-            owner, count = phase_owner(phase)
-            weight = jnp.concatenate([down_q[owner + i] for i in range(count)], axis=1)
-            step(weight, phase_columns(phase))
+        _, first, count = phases[phase]
+        return pl.ds(pl.multiple_of(phase_base(phase) * size + first, count), count)
+
+    def phase_weight(phase):
+        _, first, count = phases[phase]
+        base = phase_base(phase)
+        if count == 2 * size:
+            return jnp.concatenate([down_q[base], down_q[base + 1]], axis=1)
+        return down_q[base + first // size, :, pl.ds(first % size, count)]
 
     def tp_copy(phase, k, count=1):
         b, at = min(phase, 1), (pl.ds(k, count), slice(None), phase_columns(phase))
-        recv_sem = tp_recv.at[phase, 0 if k == 3 else 1]
+        recv_sem = tp_recv.at[phase % 2, 0 if k == 3 else 1]
         return m.copy(tp_out.at[(b, *at)], tp_in.at[(b, *at)], m.to_tp, tp_send.at[b], recv_sem)
 
     def x_copy(phase, k, low):
@@ -310,47 +334,73 @@
         at = pl.ds(0, length // 2) if low else pl.ds(length // 2, length // 2)
         to_rep = k == 2 or (k == 3 and low)
         there = (b, k - 1, at, columns_at)
-        recv_sem = x_first.at[phase, low] if k == 3 else x_last.at[b]
+        recv_sem = x_first.at[phase] if k == 3 else x_last.at[b]
         return m.copy(x_out.at[there], x_in.at[there], m.peers[2 if to_rep else 1], x_send.at[b], recv_sem)
 
-    def far_sums(phase, far):
-        b = min(phase, 1)
+    def direct_copy(phase, k):
+        there = (1, k - 1, slice(None), phase_columns(phase))
+        return m.copy(x_out.at[there], x_in.at[there], m.peers[k], x_send.at[1], x_last.at[2])
+
+    def received(ref, sem):
+        m.copy(ref, ref, m.peers[1], x_send.at[0], sem).wait_recv()
+
+    def far_sums(k):
+        def step(weight, at):
+            product = jnp.dot(activated[k, far_at, :], weight, preferred_element_type=f32)
+            tp_out[0, k, :, at] = product.astype(bf16)
+
+        tile_loop(step)
+        tp_copy(0, k).start()
+
+    def near_sums(k):
+        def step(weight, at):
+            part = jnp.dot(activated[k, near_at, :], weight, preferred_element_type=f32)
+            part = part + tp_in[0, k, :, at].astype(f32)
+            if k == 0:
+                total[0, :, at] = part
+            else:
+                x_out[0, k - 1, :, at] = part.astype(bf16)
+
+        tile_loop(step)
+        if k == 3:
+            x_copy(0, 3, 1).start()
+            x_copy(0, 3, 0).start()
+        elif k:
+            x_copy(0, k, k - 1).start()
+
+    def ffn_far_sums(phase):
+        _, _, count = phases[phase]
+        product = jnp.dot(
+            hidden[1 - m.tp].reshape(4 * length, units), phase_weight(phase), preferred_element_type=f32
+        )
+        tp_out[1, :, :, phase_columns(phase)] = product.astype(bf16).reshape(4, length, count)
+        tp_copy(phase, 3).start()
+        tp_copy(phase, 0, 3).start()
+
+    def ffn_near_sums(phase):
+        at = phase_columns(phase)
+        parts = jnp.dot(hidden[m.tp].reshape(4 * length, units), phase_weight(phase), preferred_element_type=f32)
+        tp_copy(phase, 3).wait_recv()
         for k in (3, 2, 1, 0):
-
-            def step(weight, at):
-                product = jnp.dot(far(k), weight, preferred_element_type=f32)
-                tp_out[b, k, :, at] = product.astype(bf16)
-
-            for_columns(phase, step)
-            tp_copy(phase, k).start()
-
-    def near_sums(phase, near):
-        b = min(phase, 1)
-        for k in (3, 2, 1, 0):
-            if k == 3:
-                tp_copy(phase, 3).wait_recv()
-            elif k == 2:
+            if k == 2:
                 tp_copy(phase, 0, 3).wait_recv()
-
-            def step(weight, at):
-                part = jnp.dot(near(k), weight, preferred_element_type=f32)
-                part = part + tp_in[b, k, :, at].astype(f32)
-                if k == 0:
-                    total[b, :, at] = part
-                else:
-                    x_out[b, k - 1, :, at] = part.astype(bf16)
-
-            for_columns(phase, step)
-            if k == 3:
+            part = parts[k * length : (k + 1) * length] + tp_in[1, k, :, at].astype(f32)
+            if k == 0:
+                total[1, :, at] = part
+                continue
+            x_out[1, k - 1, :, at] = part.astype(bf16)
+            if phase in direct:
+                direct_copy(phase, k).start()
+            elif k == 3:
                 x_copy(phase, 3, 1).start()
                 x_copy(phase, 3, 0).start()
-            elif k:
+            else:
                 x_copy(phase, k, k - 1).start()
 
     def forward_sums(phase):
         b, columns_at = min(phase, 1), phase_columns(phase)
+        received(x_in.at[b, 2, :, columns_at], x_first.at[phase])
         for k, low in ((1, 1), (2, 0)):
-            x_copy(phase, 3, low).wait_recv()
             first = 0 if low else length // 2
 
             def add(i, _):
@@ -363,10 +413,6 @@
             lax.fori_loop(0, length // (2 * high), add, 0)
             x_copy(phase, k, low).start()
 
-    def sums_arrived(b):
-        both = x_in.at[b, pl.ds(0, 2)]
-        m.copy(both, both, m.peers[1], x_send.at[b], x_last.at[b]).wait_recv()
-
     def sums_sent(b):
         m.copy(tp_out.at[b], tp_out.at[b], m.to_tp, tp_send.at[b], x_last.at[b]).wait_send()
         m.copy(x_out.at[b], x_out.at[b], m.peers[1], x_send.at[b], x_last.at[b]).wait_send()
@@ -377,14 +423,21 @@
             part = part + x_in[b, k - 1, at, :].astype(f32)
         return part
 
-    far_sums(0, lambda k: activated[k, far_at, :])
-    near_sums(0, lambda k: activated[k, near_at, :])
+    far_sums(3)
+    far_sums(2)
+    tp_copy(0, 3).wait_recv()
+    near_sums(3)
+    far_sums(1)
+    far_sums(0)
+    tp_copy(0, 0, 3).wait_recv()
+    for k in (2, 1, 0):
+        near_sums(k)
     m.push(FFN, 0, 2)
     forward_sums(0)
     m.push(FFN, 1, 2)
     m.pair_copy(DOWN).start()
     gather.sent()
-    sums_arrived(0)
+    received(x_in.at[0, pl.ds(0, 2)], x_last.at[0])
 
     def norm_rows(i, _):
         at = pl.ds(pl.multiple_of(i * high, high), high)
@@ -399,8 +452,8 @@
     for s in range(3, m.ring):
         for p in (0, 1):
             m.push(FFN, p, s)
-            if s == 3 and p == 0:
-                gather.forward()
+        if s == 3:
+            gather.forward()
     if m.ring < 4:
         gather.forward()
     for p in (0, 1):
@@ -414,39 +467,58 @@
         at = pl.ds(2 * i, 2)
         block = rows[at].reshape(2 * length, width)
         both = jnp.dot(block, ffn_q[...], preferred_element_type=f32)
-        hidden[at] = (jax.nn.silu(both[:, :units]) * both[:, units:]).astype(bf16).reshape(2, length, -1)
+        block = (jax.nn.silu(both[:, :units]) * both[:, units:]).astype(bf16)
+        hidden[0, i] = block[:length]
+        hidden[1, i] = block[length:]
         return _
 
     lax.fori_loop(0, 4, feed, 0)
     m.push(DOWN, 0, 2)
-    for phase in range(1, len(phases)):
-        t, p = phases[phase]
-        for q in (0, 1) if p is None else (p,):
-            if t == m.ring - 1:
-                m.ring_copy(DOWN, q, t).wait_recv()
-            elif t and (t, q) != (1, 0):
-                m.push(DOWN, q, t + 1)
-        far_sums(phase, lambda k: hidden[2 * k + 1 - m.tp])
-        near_sums(phase, lambda k: hidden[2 * k + m.tp])
-        if phase > 1:
+    for phase in range(1, final + 1):
+        t, first, count = phases[phase]
+        if t == last_t:
+            if first < size:
+                m.ring_copy(DOWN, 0, t).wait_recv()
+            if first >= size or count > size:
+                for i in range(m.pieces) if count > size else ((first - size) // 128,):
+                    m.piece_copy(i).wait_recv()
+        elif t == 1:
+            m.push(DOWN, 1, 2)
+        elif t:
+            for p in (0, 1):
+                m.push(DOWN, p, t + 1)
+        ffn_far_sums(phase)
+        ffn_near_sums(phase)
+        if phase > 1 and phase - 1 not in direct:
             forward_sums(phase - 1)
-    forward_sums(len(phases) - 1)
-    sums_arrived(1)
-
-    def finish(i, _):
-        at = pl.ds(pl.multiple_of(i * high, high), high)
-        finished[at, :] = (middle[at, :].astype(f32) + all_sums(1, at)).astype(bf16)
+    count = final_count
+    blocks = width // count
+    final_block = (phase_base(final) * size + phases[direct[0]][1]) // count
+    before_final = pl.ds(0, width - count)
+    received(x_in.at[1, pl.ds(0, 2), :, before_final], x_last.at[1])
+
+    def finish(block, parts):
+        at = pl.ds(pl.multiple_of(block * count, count), count)
+        done = middle[:, at].astype(f32) + total[1, :, at]
+        for k in range(parts):
+            done = done + x_in[1, k, :, at].astype(f32)
+        finished[:, at] = done.astype(bf16)
+        pltpu.make_async_copy(finished.at[:, at], result.at[:, at], end_sem).start()
+
+    def finish_others(j, _):
+        finish((final_block + j) % blocks, 2)
         return _
 
-    lax.fori_loop(0, length // high, finish, 0)
-    leave = pltpu.make_async_copy(finished, result, end_sem)
-    leave.start()
+    lax.fori_loop(1, blocks, finish_others, 0)
+    final_columns = pl.ds(pl.multiple_of(final_block * count, count), count)
+    received(x_in.at[1, :, :, final_columns], x_last.at[2])
+    finish(final_block, 3)
     gather.sent()
     for b in (0, 1):
         sums_sent(b)
     for w in (MODULE, OUT, FFN, DOWN):
         m.sent(w)
-    leave.wait()
+    pltpu.make_async_copy(finished, result, end_sem).wait()
 
 
 def body(
@@ -506,7 +578,7 @@
             pltpu.VMEM((8, length, width), bf16),
             pltpu.VMEM((4, 2 * length + 2 * pad, channels), f32),
             pltpu.VMEM((4, 2 * length, channels), bf16),
-            pltpu.VMEM((8, length, units), bf16),
+            pltpu.VMEM((2, 4, length, units), bf16),
             pltpu.VMEM((length, width), bf16),
             pltpu.VMEM((2, length, width), f32),
             pltpu.VMEM((2, 4, length, width), bf16),
@@ -515,9 +587,9 @@
             pltpu.VMEM((2, 3, length, width), bf16),
             pltpu.VMEM((length, width), bf16),
         ]
-        + [sem((4,)), sem((4, 2, ring - 1)), sem((4,))]
-        + [sem, sem((11,)), sem((2,)), sem((ring + 2, 2)), sem((2,)), sem((ring + 2, 2)), sem((2,))]
-        + [sem((4,)), sem((4,)), sem((5,)), sem],
+        + [sem((4,)), sem((4, 2, ring - 1)), sem((max(1, down_weight.shape[1] // 128),)), sem((4,))]
+        + [sem, sem((11,)), sem((2,)), sem((2, 2)), sem((2,)), sem((ring + 1 + down_weight.shape[1] // 128,))]
+        + [sem((3,)), sem((4,)), sem((5,)), sem],
         compiler_params=pltpu.CompilerParams(
             collective_id=0, has_side_effects=True, vmem_limit_bytes=60 * 1024 * 1024
         ),

time: 121 us -> 119 us (0.983)
  Pallas kernels: 119 us -> 117 us
    pallas_call x1, Pallas kernels: 119 us -> 117 us  [body(): pl.pallas_call(functools.partial(layer_kernel, n_rep, n_fs), out_shape=ja...]
where the time goes in v3:
time: 119 us; the launch traced here: 118 us
  Pallas kernels  117 us (98%)
  local copies, waits for them, and re-layouts  1.88 us (2%)
    pallas_call x1, Pallas kernels, body(): pl.pallas_call(functools.partial(layer_kernel, n_rep, n_fs), out_shape=ja...  117 us

profile of v3, /device:TPU:0, one launch (start us, length us, event | category | flops | bytes accessed | tf_op | source)
XLA Modules:
  0.0 118.4 jit_solution(18069924946409313197)
XLA Ops:
  0.0 116.5 %shard_map.109 = bf16[128,2048]{1,0:T(8,128)(2,1)} custom-call(bf16[128,2048]{1,0:T(8,128)(2,1)} %bitcast.6, f32[1,2048]{1,0:T(1,128)} %bitcast.7, bf16[256,512]{1,0:T(8,128)(2,1)} %value.1, bf16[256,512]{1,0:T(8,128)(2,1)} %gate.1, f32[31,512]{1,0:T(8,128)} %taps_in.1, f32[1,512]{1,0:T(1,128)} %bitcast.9, bf16[512,256]{1,0:T(8,128)(2,1)} %out.1, ...), custom_call_target="tpu_custom_call" | custom-call | tf_op jit(solution)/shard_map/pallas_call | solution.py:558
  116.5 1.9 %copy.13 = bf16[128,1,2048]{2,0,1:T(8,128)(2,1)} copy(bf16[128,1,2048]{2,0,1:T(8,128)(2,1)} %bitcast.5) | data formatting | bytes 1048576

commit v4 on v3

--- a/solution.py
+++ b/solution.py
@@ -27,25 +27,38 @@
     def __init__(self, n_rep, n_fs, sources, wholes, axes, sems):
         self.rep, self.fs, self.tp = lax.axis_index("rep"), lax.axis_index("fs"), lax.axis_index("tp")
         rep, fs, tp = self.rep, self.fs, self.tp
-        self.n_fs, self.ring = n_fs, n_fs // 2
+        self.n_fs, self.line = n_fs, n_fs // 2
         self.pair, self.place = fs % 2, fs // 2
         flip = fs + 1 - 2 * self.pair
         self.to_tp = (rep, fs, 1 - tp)
         self.peers = (None, (rep, flip, tp), (1 - rep, fs, tp), (1 - rep, flip, tp))
-        self.after = (rep, (fs + 2) % n_fs, tp)
-        self.before = (rep, (fs + n_fs - 2) % n_fs, tp)
+        self.ends = ((rep, (fs + 2) % n_fs, tp), (rep, (fs + n_fs - 2) % n_fs, tp))
+        self.has = (self.place < self.line - 1, self.place > 0)
         self.quarter = rep * 2 + self.pair
         self.other = rep * 2 + 1 - self.pair
         self.sources, self.wholes, self.axes = sources, wholes, axes
-        self.send, self.ring_recv, self.piece_recv, self.pair_recv = sems
+        self.send, self.line_recv, self.down_recv, self.pair_recv = sems
         self.pieces = max(1, wholes[DOWN].shape[2] // 128)
 
     def greet(self):
-        for device in self.peers[1:] + (self.to_tp, self.after, self.before):
+        def signal(device):
             pl.semaphore_signal(pltpu.get_barrier_semaphore(), inc=1, device_id=device, device_id_type=MESH)
 
+        for side in (0, 1):
+            pl.when(self.has[side])(functools.partial(signal, self.ends[side]))
+        for device in self.peers[1:] + (self.to_tp,):
+            signal(device)
+
     def meet(self):
-        pl.semaphore_wait(pltpu.get_barrier_semaphore(), 6)
+        inside = jnp.logical_and(*self.has)
+
+        @pl.when(inside)
+        def _():
+            pl.semaphore_wait(pltpu.get_barrier_semaphore(), 6)
+
+        @pl.when(jnp.logical_not(inside))
+        def _():
+            pl.semaphore_wait(pltpu.get_barrier_semaphore(), 5)
 
     def part(self, w, quarter):
         size = self.sources[w].shape[self.axes[w]] // 4
@@ -70,47 +83,70 @@
 
     def pair_copy(self, w):
         source, there = self.sources[w].at[self.part(w, self.other)], self.wholes[w].at[self.slots(w, self.fs)]
-        return self.copy(source, there, self.peers[1], self.send.at[w], self.pair_recv.at[w])
-
-    def piece_copy(self, i):
-        columns = self.wholes[DOWN].shape[2] // self.pieces
-        owner = ((self.place + 2) % self.ring) * 2 + 1
-        there = self.wholes[DOWN].at[owner, :, pl.ds(i * columns, columns)]
-        recv_sem = self.piece_recv.at[i]
-        return self.copy(there, there, self.after, self.send.at[DOWN], recv_sem)
-
-    def ring_copy(self, w, p, s):
-        parity = p if w == DOWN else self.pair if p == 0 else 1 - self.pair
-        owner = ((self.place + self.ring + 1 - s) % self.ring) * 2 + parity
-        there = self.wholes[w].at[self.slots(w, owner)]
-        here = self.sources[w].at[self.part(w, self.quarter)] if w != DOWN and s == 1 and p == 0 else there
-        return self.copy(here, there, self.after, self.send.at[w], self.ring_recv.at[w, p, s - 1])
+        return self.copy(source, there, self.peers[1], self.send.at[w, 2], self.pair_recv.at[w])
+
+    def line_copy(self, w, p, owner, side, own=False):
+        if w == DOWN:
+            there = self.wholes[w].at[owner * 2 + min(p, 1)]
+            if p:
+                columns = there.shape[1] // self.pieces
+                there = there.at[:, pl.ds((p - 1) * columns, columns)]
+            recv_sem = self.down_recv.at[p, owner]
+        else:
+            parity = self.pair if p == 0 else 1 - self.pair
+            there = self.wholes[w].at[self.slots(w, owner * 2 + parity)]
+            recv_sem = self.line_recv.at[w, p, owner]
+        here = self.sources[w].at[self.part(w, self.quarter)] if own and w != DOWN and p == 0 else there
+        return self.copy(here, there, self.ends[side], self.send.at[w, side], recv_sem)
 
     def push_own_ffn(self, lead):
         rows = self.sources[FFN].shape[0]
         at = pl.ds(0, rows // 4) if lead else pl.ds(rows // 4, rows - rows // 4)
         there = self.wholes[FFN].at[self.slots(FFN, self.fs)].at[at, :]
         here = self.sources[FFN].at[self.part(FFN, self.quarter)].at[at, :]
-        self.copy(here, there, self.after, self.send.at[FFN], self.ring_recv.at[FFN, 0, 0]).start()
+        for side in (0, 1):
+            copy = self.copy(here, there, self.ends[side], self.send.at[FFN, side], self.line_recv.at[FFN, 0, self.place])
+            pl.when(self.has[side])(copy.start)
 
     def push(self, w, p, s):
-        if s > 1:
-            self.ring_copy(w, p, s - 1).wait_recv()
-        elif p == (0 if w == DOWN else 1):
-            self.pair_copy(w).wait_recv()
-        if (w, p, s) == (DOWN, 1, self.ring - 1):
-            for i in range(self.pieces):
-                self.piece_copy(i).start()
-        else:
-            self.ring_copy(w, p, s).start()
+        if s == 1:
+            if p == (0 if w == DOWN else 1):
+                self.pair_copy(w).wait_recv()
+            for side in (0, 1):
+                pl.when(self.has[side])(self.line_copy(w, p, self.place, side, True).start)
+            return
+        for side in (0, 1):
+            owner = self.place - (s - 1) if side == 0 else self.place + (s - 1)
+
+            @pl.when((owner >= 0) if side == 0 else (owner < self.line))
+            def _():
+                copy = self.line_copy(w, p, owner, side)
+                copy.wait_recv()
+                pl.when(self.has[side])(copy.start)
 
     def arrived(self, w):
         for p in (0, 1):
-            self.ring_copy(w, p, self.ring - 1).wait_recv()
-
-    def sent(self, w):
-        all_sent = self.wholes[w].at[self.slots(w, 0, self.n_fs - 1)]
-        self.copy(all_sent, all_sent, self.after, self.send.at[w], self.pair_recv.at[w]).wait_send()
+            self.push(w, p, self.line)
+
+    def nearest(self, t):
+        left, right = self.place, self.line - 1 - self.place
+        both = jnp.minimum(left, right)
+        near = self.place - (t + 1) // 2 if t % 2 else self.place + t // 2
+        far = jnp.where(right > left, self.place + (t - both), self.place - (t - both))
+        return jnp.where(t <= 2 * both, near, far)
+
+    def sent(self):
+        for w in range(4):
+            self.pair_copy(w).wait_send()
+        for place in range(self.line):
+
+            @pl.when(self.place == place)
+            def _():
+                for w in range(4):
+                    for side, count in ((0, place + 1), (1, self.line - place)):
+                        if count < self.line:
+                            shards = self.wholes[w].at[self.slots(w, 0, 2 * count)]
+                            self.copy(shards, shards, self.ends[side], self.send.at[w, side], self.pair_recv.at[w]).wait_send()
 
 
 class RowGather:
@@ -236,7 +272,7 @@
     zeros = jnp.zeros((4, pad, channels), f32)
     padded[:, pl.ds(0, pad), :] = zeros
     padded[:, pl.ds(pad + 2 * length, pad), :] = zeros
-    for s in range(2, m.ring):
+    for s in range(2, m.line):
         m.push(MODULE, 0, s)
         if s > 2:
             m.push(OUT, 0, s - 1)
@@ -246,7 +282,7 @@
             gather.forward()
             m.pair_copy(FFN).start()
     for p in (0, 1):
-        m.push(OUT, p, m.ring - 1)
+        m.push(OUT, p, m.line - 1)
     m.push_own_ffn(False)
     gather.finish()
     for w in (MODULE, OUT, FFN, DOWN):
@@ -298,7 +334,7 @@
         lax.fori_loop(0, width // tile, run, 0)
 
     size = down_q.shape[2]
-    last_t = m.ring - 1
+    last_t = m.line - 1
     phases = [None] + [(t, 0, 2 * size) for t in range(last_t)]
     if size % 128 == 0:
         phases += [(last_t, 0, size)] + [(last_t, size + c, 128) for c in range(0, size, 128)]
@@ -309,7 +345,7 @@
     final_count = sum(phases[i][2] for i in direct)
 
     def phase_base(phase):
-        return ((m.place + m.ring - phases[phase][0]) % m.ring) * 2
+        return m.nearest(phases[phase][0]) * 2
 
     def phase_columns(phase):
         if phase == 0:
@@ -449,14 +485,14 @@
     lax.fori_loop(0, length // high, norm_rows, 0)
     gather = RowGather(m, rows, row_send, row_recv)
     gather.start()
-    for s in range(3, m.ring):
+    for s in range(3, m.line):
         for p in (0, 1):
             m.push(FFN, p, s)
         if s == 3:
             gather.forward()
-    if m.ring < 4:
+    if m.line < 4:
         gather.forward()
-    for p in (0, 1):
+    for p in range(1 + m.pieces):
         m.push(DOWN, p, 1)
     gather.finish()
     for k in range(4):
@@ -476,16 +512,9 @@
     m.push(DOWN, 0, 2)
     for phase in range(1, final + 1):
         t, first, count = phases[phase]
-        if t == last_t:
-            if first < size:
-                m.ring_copy(DOWN, 0, t).wait_recv()
-            if first >= size or count > size:
-                for i in range(m.pieces) if count > size else ((first - size) // 128,):
-                    m.piece_copy(i).wait_recv()
-        elif t == 1:
-            m.push(DOWN, 1, 2)
-        elif t:
-            for p in (0, 1):
+        for p in range(1 + m.pieces):
+            begin = p if p == 0 else size + (p - 1) * size // m.pieces
+            if t and (t, p) != (1, 0) and (t < last_t or first <= begin < first + count):
                 m.push(DOWN, p, t + 1)
         ffn_far_sums(phase)
         ffn_near_sums(phase)
@@ -516,8 +545,7 @@
     gather.sent()
     for b in (0, 1):
         sums_sent(b)
-    for w in (MODULE, OUT, FFN, DOWN):
-        m.sent(w)
+    m.sent()
     pltpu.make_async_copy(finished, result, end_sem).wait()
 
 
@@ -537,7 +565,7 @@
     n_rep, n_fs, n_tp = lax.axis_size("rep"), lax.axis_size("fs"), lax.axis_size("tp")
     length, seq_count, width = tokens.shape
     assert n_rep == 2 and n_tp == 2 and n_fs % 2 == 0 and n_fs > 4 and seq_count == 1
-    ring = n_fs // 2
+    line = n_fs // 2
     kernel = conv_taps.shape[0]
     channels, units = out_weight.shape[0] // 4, down_weight.shape[0] // 4
     pad = -(-(kernel // 2) // 8) * 8
@@ -587,8 +615,8 @@
             pltpu.VMEM((2, 3, length, width), bf16),
             pltpu.VMEM((length, width), bf16),
         ]
-        + [sem((4,)), sem((4, 2, ring - 1)), sem((max(1, down_weight.shape[1] // 128),)), sem((4,))]
-        + [sem, sem((11,)), sem((2,)), sem((2, 2)), sem((2,)), sem((ring + 1 + down_weight.shape[1] // 128,))]
+        + [sem((4, 3)), sem((3, 2, line)), sem((1 + max(1, down_weight.shape[1] // 128), line)), sem((4,))]
+        + [sem, sem((11,)), sem((2,)), sem((2, 2)), sem((2,)), sem((line + 1 + down_weight.shape[1] // 128,))]
         + [sem((3,)), sem((4,)), sem((5,)), sem],
         compiler_params=pltpu.CompilerParams(
             collective_id=0, has_side_effects=True, vmem_limit_bytes=60 * 1024 * 1024

time: 119 us -> 117 us (0.983)
  Pallas kernels: 117 us -> 115 us
    pallas_call x1, Pallas kernels: 117 us -> 115 us  [body(): pl.pallas_call(functools.partial(layer_kernel, n_rep, n_fs), out_shape=ja...]
where the time goes in v4:
time: 117 us
  Pallas kernels  115 us (98%)
  local copies, waits for them, and re-layouts  1.88 us (2%)
    pallas_call x1, Pallas kernels, body(): pl.pallas_call(functools.partial(layer_kernel, n_rep, n_fs), out_shape=ja...  115 us

profile of v4, /device:TPU:0, one launch (start us, length us, event | category | flops | bytes accessed | tf_op | source)
XLA Modules:
  0.0 116.9 jit_solution(7448480611499256589)
XLA Ops:
  0.0 115.0 %shard_map.109 = bf16[128,2048]{1,0:T(8,128)(2,1)} custom-call(bf16[128,2048]{1,0:T(8,128)(2,1)} %bitcast.6, f32[1,2048]{1,0:T(1,128)} %bitcast.7, bf16[256,512]{1,0:T(8,128)(2,1)} %value.1, bf16[256,512]{1,0:T(8,128)(2,1)} %gate.1, f32[31,512]{1,0:T(8,128)} %taps_in.1, f32[1,512]{1,0:T(1,128)} %bitcast.9, bf16[512,256]{1,0:T(8,128)(2,1)} %out.1, ...), custom_call_target="tpu_custom_call" | custom-call | tf_op jit(solution)/shard_map/pallas_call | solution.py:586
  115.0 1.9 %copy.13 = bf16[128,1,2048]{2,0,1:T(8,128)(2,1)} copy(bf16[128,1,2048]{2,0,1:T(8,128)(2,1)} %bitcast.5) | data formatting | bytes 1048576

commit v5 on v4

--- a/solution.py
+++ b/solution.py
@@ -21,6 +21,20 @@
 
 
 MODULE, OUT, FFN, DOWN = range(4)
+
+
+def nearest(place, line, t):
+    left, right = place, line - 1 - place
+    both = jnp.minimum(left, right)
+    near = place - (t + 1) // 2 if t % 2 else place + t // 2
+    far = jnp.where(right > left, place + (t - both), place - (t - both))
+    return jnp.where(t <= 2 * both, near, far)
+
+
+def final_columns(place, line, size):
+    count = size if size % 128 == 0 else 2 * size
+    block = (nearest(place, line, line - 1) * 2 * size + 2 * size - count) // count
+    return block, count
 
 
 class Moves:
@@ -83,7 +97,7 @@
 
     def pair_copy(self, w):
         source, there = self.sources[w].at[self.part(w, self.other)], self.wholes[w].at[self.slots(w, self.fs)]
-        return self.copy(source, there, self.peers[1], self.send.at[w, 2], self.pair_recv.at[w])
+        return self.copy(source, there, self.peers[1], self.send.at[w, 0], self.pair_recv.at[w])
 
     def line_copy(self, w, p, owner, side, own=False):
         if w == DOWN:
@@ -91,11 +105,11 @@
             if p:
                 columns = there.shape[1] // self.pieces
                 there = there.at[:, pl.ds((p - 1) * columns, columns)]
-            recv_sem = self.down_recv.at[p, owner]
+            recv_sem = self.down_recv.at[p, owner - side]
         else:
             parity = self.pair if p == 0 else 1 - self.pair
             there = self.wholes[w].at[self.slots(w, owner * 2 + parity)]
-            recv_sem = self.line_recv.at[w, p, owner]
+            recv_sem = self.line_recv.at[w, p, owner - side]
         here = self.sources[w].at[self.part(w, self.quarter)] if own and w != DOWN and p == 0 else there
         return self.copy(here, there, self.ends[side], self.send.at[w, side], recv_sem)
 
@@ -105,15 +119,24 @@
         there = self.wholes[FFN].at[self.slots(FFN, self.fs)].at[at, :]
         here = self.sources[FFN].at[self.part(FFN, self.quarter)].at[at, :]
         for side in (0, 1):
-            copy = self.copy(here, there, self.ends[side], self.send.at[FFN, side], self.line_recv.at[FFN, 0, self.place])
-            pl.when(self.has[side])(copy.start)
+
+
+            @pl.when(self.has[side])
+            def _():
+                recv_sem = self.line_recv.at[FFN, 0, self.place - side]
+                self.copy(here, there, self.ends[side], self.send.at[FFN, side], recv_sem).start()
 
     def push(self, w, p, s):
         if s == 1:
             if p == (0 if w == DOWN else 1):
                 self.pair_copy(w).wait_recv()
             for side in (0, 1):
-                pl.when(self.has[side])(self.line_copy(w, p, self.place, side, True).start)
+
+
+                @pl.when(self.has[side])
+                def _():
+                    self.line_copy(w, p, self.place, side, True).start()
+
             return
         for side in (0, 1):
             owner = self.place - (s - 1) if side == 0 else self.place + (s - 1)
@@ -128,25 +151,17 @@
         for p in (0, 1):
             self.push(w, p, self.line)
 
-    def nearest(self, t):
-        left, right = self.place, self.line - 1 - self.place
-        both = jnp.minimum(left, right)
-        near = self.place - (t + 1) // 2 if t % 2 else self.place + t // 2
-        far = jnp.where(right > left, self.place + (t - both), self.place - (t - both))
-        return jnp.where(t <= 2 * both, near, far)
-
     def sent(self):
-        for w in range(4):
-            self.pair_copy(w).wait_send()
         for place in range(self.line):
 
             @pl.when(self.place == place)
             def _():
                 for w in range(4):
                     for side, count in ((0, place + 1), (1, self.line - place)):
-                        if count < self.line:
-                            shards = self.wholes[w].at[self.slots(w, 0, 2 * count)]
-                            self.copy(shards, shards, self.ends[side], self.send.at[w, side], self.pair_recv.at[w]).wait_send()
+                        count = (2 * count if count < self.line else 0) + 1 - side
+                        if count:
+                            shards = self.wholes[w].at[self.slots(w, 0, count)]
+                            self.copy(shards, shards, self.peers[1], self.send.at[w, side], self.pair_recv.at[w]).wait_send()
 
 
 class RowGather:
@@ -165,10 +180,10 @@
             (rows.at[first], rows.at[first], m.to_tp),
             (rows.at[near_rep], rows.at[near_rep], m.to_tp),
             (rows.at[near_pair], rows.at[near_pair], m.to_tp),
-            (rows.at[across, low], rows.at[across, low], m.to_tp),
-            (rows.at[across, high], rows.at[across, high], m.to_tp),
+            (rows.at[across], rows.at[across], m.to_tp),
         )
-        self.copies = [m.copy(*move, send_sem, recv_sems.at[i]) for i, move in enumerate(moves)]
+        self.copies = [m.copy(*move, send_sem, recv_sems.at[4 if i == 5 else i]) for i, move in enumerate(moves)]
+        self.diagonal = m.copy(rows.at[across], rows.at[across], pair, send_sem, recv_sems.at[4])
         seven = rows.at[pl.ds(0, 7)]
         self.all_sent = m.copy(seven, seven, pair, send_sem, recv_sems.at[0])
 
@@ -182,12 +197,14 @@
             self.copies[i + 4].start()
 
     def finish(self):
-        for i in (2, 3, 4, 5):
+        for i in (2, 3):
             self.copies[i].wait_recv()
             self.copies[i + 5].start()
+        self.diagonal.wait_recv()
+        self.copies[9].start()
 
     def ready(self, k):
-        for i in ((6,), (8,), (7,), (9, 10))[k]:
+        for i in ((6,), (8,), (7,), (9,))[k]:
             self.copies[i].wait_recv()
 
     def sent(self):
@@ -196,14 +213,14 @@
 
 def layer_kernel(
     n_rep, n_fs, tokens_in, mix_gain_in, value, gate, taps_in, head_gain_in, out, ffn_gain_in, ffn_gate, ffn_up,
-    down, result,
+    down, early, partial, late,
     *scratch,
 ):
     staged, wholes, scratch = scratch[:4], scratch[4:8], scratch[8:]
     module_q, out_q, ffn_q, down_q = wholes
     tokens, mix_gain, taps, head_gain, ffn_gain = scratch[:5]
-    rows_a, rows, padded, activated, hidden, middle, total, tp_out, tp_in, x_out, x_in, finished = scratch[5:17]
-    weight_sems, scratch = scratch[17:21], scratch[21:]
+    rows_a, rows, padded, activated, hidden, middle, total, tp_out, tp_in, x_out, x_in, finished, last_partial = scratch[5:18]
+    weight_sems, scratch = scratch[18:22], scratch[22:]
     row_send, row_recv, tp_send, tp_recv, x_send, x_first, x_last, stage_sem, small_sem, end_sem = scratch
     channels, units = out_q.shape[1], down_q.shape[1]
     m = Moves(n_rep, n_fs, staged, wholes, (1, 0, 1, 0), weight_sems)
@@ -342,10 +359,9 @@
         phases += [(last_t, 0, 2 * size)]
     final = len(phases) - 1
     direct = [i for i in range(1, final + 1) if phases[i][0] == last_t and (phases[i][1] or i == final)]
-    final_count = sum(phases[i][2] for i in direct)
 
     def phase_base(phase):
-        return m.nearest(phases[phase][0]) * 2
+        return nearest(m.place, m.line, phases[phase][0]) * 2
 
     def phase_columns(phase):
         if phase == 0:
@@ -374,8 +390,9 @@
         return m.copy(x_out.at[there], x_in.at[there], m.peers[2 if to_rep else 1], x_send.at[b], recv_sem)
 
     def direct_copy(phase, k):
-        there = (1, k - 1, slice(None), phase_columns(phase))
-        return m.copy(x_out.at[there], x_in.at[there], m.peers[k], x_send.at[1], x_last.at[2])
+        source = x_out.at[1, k - 1, :, phase_columns(phase)]
+        first, count = phases[phase][1] - phases[direct[0]][1], phases[phase][2]
+        return m.copy(source, late.at[k - 1, :, pl.ds(first, count)], m.peers[k], x_send.at[1], x_last.at[2])
 
     def received(ref, sem):
         m.copy(ref, ref, m.peers[1], x_send.at[0], sem).wait_recv()
@@ -520,33 +537,53 @@
         ffn_near_sums(phase)
         if phase > 1 and phase - 1 not in direct:
             forward_sums(phase - 1)
-    count = final_count
+    final_block, count = final_columns(m.place, m.line, size)
+    final_at = pl.ds(pl.multiple_of(final_block * count, count), count)
+    last_partial[...] = middle[:, final_at].astype(f32) + total[1, :, final_at]
+    keep = pltpu.make_async_copy(last_partial, partial, end_sem.at[0])
+    keep.start()
     blocks = width // count
-    final_block = (phase_base(final) * size + phases[direct[0]][1]) // count
     before_final = pl.ds(0, width - count)
     received(x_in.at[1, pl.ds(0, 2), :, before_final], x_last.at[1])
 
-    def finish(block, parts):
+    def finish(j, _):
+        block = (final_block + j) % blocks
         at = pl.ds(pl.multiple_of(block * count, count), count)
         done = middle[:, at].astype(f32) + total[1, :, at]
-        for k in range(parts):
+        for k in range(2):
             done = done + x_in[1, k, :, at].astype(f32)
         finished[:, at] = done.astype(bf16)
-        pltpu.make_async_copy(finished.at[:, at], result.at[:, at], end_sem).start()
-
-    def finish_others(j, _):
-        finish((final_block + j) % blocks, 2)
+        pltpu.make_async_copy(finished.at[:, at], early.at[:, at], end_sem.at[1]).start()
         return _
 
-    lax.fori_loop(1, blocks, finish_others, 0)
-    final_columns = pl.ds(pl.multiple_of(final_block * count, count), count)
-    received(x_in.at[1, :, :, final_columns], x_last.at[2])
-    finish(final_block, 3)
+    lax.fori_loop(1, blocks, finish, 0)
     gather.sent()
-    for b in (0, 1):
-        sums_sent(b)
+    sums_sent(0)
     m.sent()
-    pltpu.make_async_copy(finished, result, end_sem).wait()
+    others = finished.at[:, before_final]
+    pltpu.make_async_copy(others, others, end_sem.at[1]).wait()
+    keep.wait()
+    sums_sent(1)
+    received(late, x_last.at[2])
+
+
+def closing_kernel(n_fs, size, early, partial, late, result, rows, last, parts, sems):
+    block, count = final_columns(lax.axis_index("fs") // 2, n_fs // 2, size)
+    copies = [
+        pltpu.make_async_copy(source, there, sems.at[i])
+        for i, (source, there) in enumerate(((early, rows), (partial, last), (late, parts)))
+    ]
+    for copy in copies:
+        copy.start()
+    for copy in copies:
+        copy.wait()
+    done = last[...]
+    for k in range(3):
+        done = done + parts[k].astype(f32)
+    rows[:, pl.ds(pl.multiple_of(block * count, count), count)] = done.astype(bf16)
+    leave = pltpu.make_async_copy(rows, result, sems.at[3])
+    leave.start()
+    leave.wait()
 
 
 def body(
@@ -583,11 +620,14 @@
         ffn_up_weight,
         down_weight,
     )
-    layer_rows = pl.pallas_call(
+    size = down_weight.shape[1]
+    count = size if size % 128 == 0 else 2 * size
+    late_shapes = (((length, width), bf16), ((length, count), f32), ((3, length, count), bf16))
+    parts = pl.pallas_call(
         functools.partial(layer_kernel, n_rep, n_fs),
-        out_shape=jax.ShapeDtypeStruct((length, width), bf16),
+        out_shape=[jax.ShapeDtypeStruct(*shape) for shape in late_shapes],
         in_specs=[pl.BlockSpec(memory_space=pl.ANY)] * len(operands),
-        out_specs=pl.BlockSpec(memory_space=pl.ANY),
+        out_specs=[pl.BlockSpec(memory_space=pl.ANY)] * 3,
         scratch_shapes=[
             pltpu.VMEM((value_weight.shape[0], 8 * channels), bf16),
             pltpu.VMEM(out_weight.shape, bf16),
@@ -614,14 +654,23 @@
             pltpu.VMEM((2, 3, length, width), bf16),
             pltpu.VMEM((2, 3, length, width), bf16),
             pltpu.VMEM((length, width), bf16),
+            pltpu.VMEM((length, count), f32),
         ]
-        + [sem((4, 3)), sem((3, 2, line)), sem((1 + max(1, down_weight.shape[1] // 128), line)), sem((4,))]
-        + [sem, sem((11,)), sem((2,)), sem((2, 2)), sem((2,)), sem((line + 1 + down_weight.shape[1] // 128,))]
-        + [sem((3,)), sem((4,)), sem((5,)), sem],
+        + [sem((4, 2)), sem((3, 2, line - 1)), sem((1 + max(1, down_weight.shape[1] // 128), line - 1)), sem((4,))]
+        + [sem, sem((10,)), sem((2,)), sem((2, 2)), sem((2,)), sem((line + 1,))]
+        + [sem((3,)), sem((4,)), sem((5,)), sem((2,))],
         compiler_params=pltpu.CompilerParams(
             collective_id=0, has_side_effects=True, vmem_limit_bytes=60 * 1024 * 1024
         ),
     )(*operands)
+    layer_rows = pl.pallas_call(
+        functools.partial(closing_kernel, n_fs, size),
+        out_shape=jax.ShapeDtypeStruct((length, width), bf16),
+        in_specs=[pl.BlockSpec(memory_space=pl.ANY)] * 3,
+        out_specs=pl.BlockSpec(memory_space=pl.ANY),
+        scratch_shapes=[pltpu.VMEM(*shape) for shape in late_shapes] + [sem((4,))],
+        compiler_params=pltpu.CompilerParams(vmem_limit_bytes=60 * 1024 * 1024),
+    )(*parts)
     return layer_rows.reshape(length, seq_count, width)
 
 

time: 117 us -> 116 us (level)
  local copies, waits for them, and re-layouts: 1.88 us -> 0 us
    unnamed x1 -> x0, local copies, waits for them, and re-layouts: 1.88 us -> none
    pallas_call x1 -> x2, Pallas kernels: 115 us -> 116 us  [the longest x1 114 us: body(): pl.pallas_call(functools.partial(layer_kernel, n_rep, n_fs), out_shape=[j...]
where the time goes in v5:
time: 116 us
  Pallas kernels  116 us (100%)
    pallas_call x1, Pallas kernels, body(): pl.pallas_call(functools.partial(layer_kernel, n_rep, n_fs), out_shape=[j...  114 us

profile of v5, /device:TPU:0, one launch (start us, length us, event | category | flops | bytes accessed | tf_op | source)
XLA Modules:
  0.0 116.3 jit_solution(109561974737831167)
XLA Ops:
  0.0 114.3 %shard_map.109 = (bf16[128,2048]{1,0:T(8,128)(2,1)}, f32[128,256]{1,0:T(8,128)}, bf16[3,128,256]{2,1,0:T(8,128)(2,1)}) custom-call(bf16[128,2048]{1,0:T(8,128)(2,1)} %bitcast.5, f32[1,2048]{1,0:T(1,128)} %bitcast.6, bf16[256,512]{1,0:T(8,128)(2,1)} %value.1, bf16[256,512]{1,0:T(8,128)(2,1)} %gate.1, f32[31,512]{1,0:T(8,128)} %taps_in.1, f32[1,512]{1,0:T(1,128)} %bitcast.8, ...), custom_call_target="tpu_custom_call" | custom-call | tf_op jit(solution)/shard_map/pallas_call | solution.py:626
  114.3 2.0 %shard_map.110 = bf16[128,2048]{1,0:T(8,128)(2,1)} custom-call(bf16[128,2048]{1,0:T(8,128)(2,1)} %get-tuple-element.8.early, f32[128,256]{1,0:T(8,128)} %get-tuple-element.9.partial, bf16[3,128,256]{2,1,0:T(8,128)(2,1)} %get-tuple-element.10.late), custom_call_target="tpu_custom_call" | custom-call | tf_op jit(solution)/shard_map/pallas_call | solution.py:666

commit v6 on v5

--- a/solution.py
+++ b/solution.py
@@ -534,8 +534,10 @@
             if t and (t, p) != (1, 0) and (t < last_t or first <= begin < first + count):
                 m.push(DOWN, p, t + 1)
         ffn_far_sums(phase)
+        if phase == final:
+            forward_sums(direct[0] - 1)
         ffn_near_sums(phase)
-        if phase > 1 and phase - 1 not in direct:
+        if 1 < phase < direct[0]:
             forward_sums(phase - 1)
     final_block, count = final_columns(m.place, m.line, size)
     final_at = pl.ds(pl.multiple_of(final_block * count, count), count)

time: 116 us -> 116 us (level)
  no operation moved by 1% of the time
where the time goes in v6:
time: 116 us
  Pallas kernels  116 us (100%)
    pallas_call x1, Pallas kernels, body(): pl.pallas_call(functools.partial(layer_kernel, n_rep, n_fs), out_shape=[j...  114 us

profile of v6, /device:TPU:0, one launch (start us, length us, event | category | flops | bytes accessed | tf_op | source)
XLA Modules:
  0.0 116.3 jit_solution(10767377122569792660)
XLA Ops:
  0.0 114.3 %shard_map.109 = (bf16[128,2048]{1,0:T(8,128)(2,1)}, f32[128,256]{1,0:T(8,128)}, bf16[3,128,256]{2,1,0:T(8,128)(2,1)}) custom-call(bf16[128,2048]{1,0:T(8,128)(2,1)} %bitcast.5, f32[1,2048]{1,0:T(1,128)} %bitcast.6, bf16[256,512]{1,0:T(8,128)(2,1)} %value.1, bf16[256,512]{1,0:T(8,128)(2,1)} %gate.1, f32[31,512]{1,0:T(8,128)} %taps_in.1, f32[1,512]{1,0:T(1,128)} %bitcast.8, ...), custom_call_target="tpu_custom_call" | custom-call | tf_op jit(solution)/shard_map/pallas_call | solution.py:628
  114.3 2.0 %shard_map.110 = bf16[128,2048]{1,0:T(8,128)(2,1)} custom-call(bf16[128,2048]{1,0:T(8,128)(2,1)} %get-tuple-element.8.early, f32[128,256]{1,0:T(8,128)} %get-tuple-element.9.partial, bf16[3,128,256]{2,1,0:T(8,128)(2,1)} %get-tuple-element.10.late), custom_call_target="tpu_custom_call" | custom-call | tf_op jit(solution)/shard_map/pallas_call | solution.py:668
